TPU v7x, 32 devices: a whole 2x2x4 slice. The times are simulated.
32 devices in a mesh: fs: 8 (over z, y), tp: 4 (over x, core).
Axes of the slice: x: 2, y: 2, z: 4, core: 2. Of those that a mesh axis runs over, the one named last changes fastest.
Arguments:
- stream: bfloat16 [3072, 2048], P('fs', 'tp'), may hold values from -3 to 3
- gain_first: float32 [2048], replicated, may hold values from 0.1 to 1.9
- gain_mixer: float32 [2048], replicated, may hold values from 0.1 to 1.9
- gain_second: float32 [2048], replicated, may hold values from 0.1 to 1.9
- gate_weight: float32 [2048, 5632], P('fs', 'tp'), may hold values from -0.125 to 0.125
- gate_scale: float32 [5632], P('tp'), may hold values from 0.5 to 2
- up_weight: float32 [2048, 5632], P('fs', 'tp'), may hold values from -0.125 to 0.125
- up_scale: float32 [5632], P('tp'), may hold values from 0.5 to 2
- down_weight: float32 [5632, 2048], P('tp', 'fs'), may hold values from -0.109375 to 0.109375
- down_scale: float32 [2048], P('tp'), may hold values from 0.5 to 2
- pool_in_weight: float32 [2048, 512], P('fs', 'tp'), may hold values from -0.125 to 0.125
- pool_in_scale: float32 [512], P('tp'), may hold values from 0.5 to 2
- pool_out_weight: float32 [512, 2048], P('tp', 'fs'), may hold values from -0.375 to 0.375
- pool_out_scale: float32 [2048], P('tp'), may hold values from 0.5 to 2
Outputs:
- layer_out: bfloat16 [3072, 2048], P('fs', 'tp')
All inputs are finite; a program needn't handle non-finite values.
Results may differ from a plain program's by a relative error of at most 0.025.
Values may be sent and summed in bfloat16 or wider, within the bound.
A program may use at most 64 MiB of HBM per device.

v0:
```python
import functools

import jax
import jax.numpy as jnp
from jax import lax
from jax.experimental import pallas as pl
from jax.experimental.pallas import tpu as pltpu
from jax.sharding import PartitionSpec as P

SEQ = 128
MESH = pl.DeviceIdType.MESH

eps = 1e-06
WINDOWS = (2, 4, 8, 16)


def fs_grid(count):
    ny = 1
    while (2 * ny) * (2 * ny) <= count and count % (2 * ny) == 0:
        ny *= 2
    return ny, count // ny


def grid_shape(row_blocks, col_blocks, block):
    rows, cols = block
    if cols % 128 == 0:
        return (row_blocks * rows, col_blocks * cols)
    return (row_blocks, col_blocks, rows, cols)


def place(whole, block, row_block, col_block, part=(0, None)):
    rows, cols = block
    first, count = part[0], rows if part[1] is None else part[1]
    if len(whole.shape) == 2:
        return whole.at[
            pl.ds(pl.multiple_of(row_block * rows + first, 16), count),
            pl.ds(pl.multiple_of(col_block * cols, 128), cols),
        ]
    return whole.at[row_block, col_block, pl.ds(first, count)]


def flat(whole):
    if whole.ndim == 2:
        return whole
    return whole.transpose(0, 2, 1, 3).reshape(whole.shape[0] * whole.shape[2], -1)


def gather_kernel(nfs, ntp, pool_in, pool_out, gate, up, down, stream, scales,
                  in_all, out_all, gate_all, up_all, down_all, stream_all, scales_all,
                  send_sem, recv_sem, local_sem, tsend, trecv, psend, precv, ssend, srecv):
    ny, nz = fs_grid(nfs)
    nx = ntp // 2
    fs, tp = lax.axis_index("fs"), lax.axis_index("tp")
    z, y = fs // ny, fs % ny
    x, core = tp // 2, tp % 2
    partner = x * 2 + (1 - core)
    alternate = ny == 2 and nz > 1

    barrier = pltpu.get_barrier_semaphore()

    def greet(cond, f, t):
        @pl.when(cond)
        def _():
            pl.semaphore_signal(barrier, inc=1, device_id={"fs": f, "tp": t}, device_id_type=MESH)

    greet(z > 0, fs - ny, tp)
    greet(z < nz - 1, fs + ny, tp)
    greet(y > 0, fs - 1, tp)
    greet(y < ny - 1, fs + 1, tp)
    for k in range(1, ntp):
        pl.semaphore_signal(
            barrier, inc=1, device_id={"fs": fs, "tp": (tp + k) % ntp}, device_id_type=MESH
        )
    peers = ntp - 1
    for cond in (z > 0, z < nz - 1, y > 0, y < ny - 1):
        peers = peers + jnp.where(cond, 1, 0)
    pl.semaphore_wait(barrier, peers)

    pieces = [
        (lambda: pool_in, lambda f: place(in_all, pool_in.shape, f, tp)),
        (lambda: pool_out, lambda f: place(out_all, pool_out.shape, tp, f)),
    ]
    npool = len(pieces)
    for own, whole, by_rows in ((gate, gate_all, True), (up, up_all, True), (down, down_all, False)):
        rows = own.shape[0]
        halves = 2 if alternate else 1
        for h in range(halves):
            part = (h * (rows // halves), rows // halves)

            def own_part(own=own, part=part):
                return own.at[pl.ds(*part)]

            def whole_part(f, own=own, whole=whole, part=part, by_rows=by_rows):
                return place(whole, own.shape, f if by_rows else 0, 0 if by_rows else f, part)

            pieces.append((own_part, whole_part))
    started = []

    def remote(piece, f, direction, target, mine=False):
        own, whole = pieces[piece]
        return pltpu.make_async_remote_copy(
            src_ref=own() if mine else whole(f),
            dst_ref=whole(f),
            send_sem=send_sem.at[piece, f, direction],
            recv_sem=recv_sem.at[piece, f],
            device_id={"fs": target, "tp": tp},
            device_id_type=MESH,
        )

    def send(cond, piece, f, direction, mine=False):
        target = fs + (-ny, ny, -1, 1)[direction]

        @pl.when(cond)
        def _():
            remote(piece, f, direction, target, mine).start()

        started.append((cond, piece, f, direction, target, mine))

    def arrived(cond, piece, f):
        @pl.when(cond)
        def _():
            remote(piece, f, 0, fs, False).wait_recv()

    def by_y(cond, piece, f, mine=False):
        send(cond & (y > 0), piece, f, 2, mine)
        send(cond & (y < ny - 1), piece, f, 3, mine)

    yes = z >= 0

    def stream_place(slot):
        return place(stream_all, stream.shape, 0, slot)

    def stream_copy(src, slot, t_target, k):
        return pltpu.make_async_remote_copy(
            src_ref=src, dst_ref=stream_place(slot), send_sem=tsend.at[k], recv_sem=trecv.at[slot],
            device_id={"fs": fs, "tp": t_target}, device_id_type=MESH)

    def slab(which, slot):
        if which == 0:
            if len(in_all.shape) == 2:
                cols = pool_in.shape[1]
                return in_all.at[:, pl.ds(pl.multiple_of(slot * cols, 128), cols)]
            return in_all.at[:, slot]
        if len(out_all.shape) == 2:
            rows = pool_out.shape[0]
            return out_all.at[pl.ds(pl.multiple_of(slot * rows, 16), rows)]
        return out_all.at[slot]

    def pool_copy(which, slot, t_target, k):
        return pltpu.make_async_remote_copy(
            src_ref=slab(which, slot), dst_ref=slab(which, slot),
            send_sem=psend.at[which, k], recv_sem=precv.at[which, slot],
            device_id={"fs": fs, "tp": t_target}, device_id_type=MESH)

    def scale_copy(k, slot, t_target):
        return pltpu.make_async_remote_copy(
            src_ref=scales, dst_ref=scales_all.at[slot], send_sem=ssend.at[k], recv_sem=srecv.at[slot],
            device_id={"fs": fs, "tp": t_target}, device_id_type=MESH)

    npieces = len(pieces)
    locals_ = [pltpu.make_async_copy(own(), whole(fs), local_sem.at[i]) for i, (own, whole) in enumerate(pieces)]
    locals_.append(pltpu.make_async_copy(stream, stream_place(tp), local_sem.at[npieces]))
    locals_.append(pltpu.make_async_copy(scales, scales_all.at[tp], local_sem.at[npieces + 1]))
    for piece in range(npieces):
        send(z > 0, piece, fs, 0, True)
        send(z < nz - 1, piece, fs, 1, True)
        by_y(yes, piece, fs, True)
    stream_sends = []
    for k in range(1, nx):
        stream_sends.append(stream_copy(stream, tp, (x + k) % nx * 2 + core, k - 1))
    stream_sends.append(stream_copy(stream, tp, partner, nx - 1))
    stream_sends += [scale_copy(k - 1, tp, (tp + k) % ntp) for k in range(1, ntp)]
    for copy in stream_sends:
        copy.start()
    for copy in locals_:
        copy.start()

    def row_arrivals(piece, d, alt):
        low, high = fs - d * ny, fs + d * ny
        has_low, has_high = z >= d, z + d <= nz - 1
        for cond, f, direction, ahead, end in (
            (has_low, low, 1, z < nz - 1, z == d),
            (has_high, high, 0, z > 0, z + d == nz - 1),
        ):
            arrived(cond, piece, f)
            send(cond & ahead, piece, f, direction)
            if alt:
                by_y(cond & jnp.logical_not(end), piece, f)
                other = f + 1 - 2 * y
                arrived(cond & end, piece, other)
                send(cond & end & ahead, piece, other, direction)
            else:
                by_y(cond, piece, f)

    def column_arrivals(piece, alt):
        for d in range(nz):
            for sign in ((1,) if d == 0 else (-1, 1)):
                row_ok = (z + sign * d >= 0) & (z + sign * d <= nz - 1)
                if alt:
                    at = z + sign * d
                    if d == 0:
                        continue
                    row_ok = row_ok & (at != 0) & (at != nz - 1)
                base = fs + sign * d * ny
                for e in range(1, ny):
                    for step, direction, ok, ahead in (
                        (-e, 3, y >= e, y < ny - 1),
                        (e, 2, y + e <= ny - 1, y > 0),
                    ):
                        arrived(row_ok & ok, piece, base + step)
                        if ny > 2:
                            send(row_ok & ok & ahead, piece, base + step, direction)

    is_alt = [alternate and p >= npool and p % 2 == 1 for p in range(npieces)]

    for d in range(1, nz):
        for p in range(npool):
            row_arrivals(p, d, False)
    pool_sends = []
    for p in range(npool):
        column_arrivals(p, False)
        locals_[p].wait()
        pool_sends += [pool_copy(p, tp, (x + k) % nx * 2 + core, k - 1) for k in range(1, nx)]
        pool_sends.append(pool_copy(p, tp, partner, nx - 1))
    for copy in pool_sends:
        copy.start()
    for k in range(1, nx):
        slot = (x + k) % nx * 2 + core
        stream_copy(stream, slot, partner, 0).wait_recv()
        copy = stream_copy(stream_place(slot), slot, partner, nx - 1 + k)
        copy.start()
        stream_sends.append(copy)

    for p in range(npieces):
        if is_alt[p]:
            other = fs + 1 - 2 * y
            arrived(yes, p, other)
            send(z == 0, p, other, 1)
            send(z == nz - 1, p, other, 0)
    for d in range(1, nz):
        for p in range(npool, npieces):
            row_arrivals(p, d, is_alt[p])
        if d == 1:
            for k in range(1, nx):
                slot = (x + k) % nx * 2 + core
                for p in range(npool):
                    pool_copy(p, slot, partner, 0).wait_recv()
                    copy = pool_copy(p, slot, partner, nx - 1 + k)
                    copy.start()
                    pool_sends.append(copy)
    for p in range(npool, npieces):
        column_arrivals(p, is_alt[p])
    for k in range(nx):
        slot = (x + k) % nx * 2 + (1 - core)
        stream_copy(stream, slot, partner, 0).wait_recv()
        for p in range(npool):
            pool_copy(p, slot, partner, 0).wait_recv()
    for k in range(1, ntp):
        scale_copy(0, (tp + k) % ntp, partner).wait_recv()
    for copy in locals_[npool:]:
        copy.wait()
    for copy in stream_sends + pool_sends:
        copy.wait_send()
    for cond, piece, f, direction, target, mine in started:
        @pl.when(cond)
        def _():
            remote(piece, f, direction, target, mine).wait_send()


def gather_all(nfs, ntp, pool_in, pool_out, gate, up, down, stream, scales):
    ny, nz = fs_grid(nfs)
    nx = ntp // 2
    npieces = 8 if (ny == 2 and nz > 1) else 5
    any_spec = pl.BlockSpec(memory_space=pl.ANY)
    shapes = (
        grid_shape(nfs, ntp, pool_in.shape),
        grid_shape(ntp, nfs, pool_out.shape),
        grid_shape(nfs, 1, gate.shape),
        grid_shape(nfs, 1, up.shape),
        grid_shape(1, nfs, down.shape),
        grid_shape(1, ntp, stream.shape),
    )
    dma = pltpu.SemaphoreType.DMA
    return pl.pallas_call(
        functools.partial(gather_kernel, nfs, ntp),
        name="collect_weights",
        out_shape=tuple(jax.ShapeDtypeStruct(shape, jnp.bfloat16) for shape in shapes)
        + (jax.ShapeDtypeStruct((ntp,) + scales.shape, jnp.float32),),
        in_specs=[any_spec] * 7,
        out_specs=[any_spec] * 7,
        scratch_shapes=[
            dma((npieces, nfs, 4)),
            dma((npieces, nfs)),
            dma((npieces + 2,)),
            dma((2 * nx,)),
            dma((ntp,)),
            dma((2, 2 * nx)),
            dma((2, ntp)),
            dma((ntp,)),
            dma((ntp,)),
        ],
        compiler_params=pltpu.CompilerParams(collective_id=0, has_side_effects=True, vmem_limit_bytes=1 << 20),
    )(pool_in, pool_out, gate, up, down, stream, scales)


def sum_kernel(ntp, gathers, pieces, partial, resid, scale, out, pair, pair_sum, cross, *sems):
    pair_send, pair_recv, cross_send, cross_recv = sems[:4]
    nx = ntp // 2
    tp, fs = lax.axis_index("tp"), lax.axis_index("fs")
    x, core = tp // 2, tp % 2
    partner = x * 2 + (1 - core)
    rows, width = resid.shape
    step = rows // pieces
    barrier = pltpu.get_barrier_semaphore()
    pl.semaphore_signal(barrier, inc=1, device_id={"fs": fs, "tp": partner}, device_id_type=MESH)
    for k in range(1, nx):
        pl.semaphore_signal(
            barrier, inc=1, device_id={"fs": fs, "tp": (x + k) % nx * 2 + core}, device_id_type=MESH
        )
    pl.semaphore_wait(barrier, nx)

    def remote(src, dst, send, recv, target):
        return pltpu.make_async_remote_copy(
            src_ref=src, dst_ref=dst, send_sem=send, recv_sem=recv,
            device_id={"fs": fs, "tp": target}, device_id_type=MESH)

    def columns(t):
        return pl.ds(pl.multiple_of(t * width, width), width)

    parts = [pl.ds(i * step, step) for i in range(pieces)]
    offsets = list(range(1, nx)) + [0]
    sends = []
    for k in offsets:
        for i, part in enumerate(parts):
            copy = remote(partial.at[part, columns((x + k) % nx * 2 + (1 - core))], pair.at[k, part],
                          pair_send.at[k, i], pair_recv.at[k, i], partner)
            copy.start()
            sends.append(copy)
    for k in offsets[:-1]:
        target = (x + k) % nx * 2 + core
        for i, part in enumerate(parts):
            remote(pair.at[k, part], pair.at[k, part], pair_send.at[k, i], pair_recv.at[k, i], partner).wait_recv()
            pair_sum[k - 1, part] = (
                partial[part, columns(target)].astype(jnp.float32) + pair[k, part].astype(jnp.float32)
            ).astype(jnp.bfloat16)
            copy = remote(pair_sum.at[k - 1, part], cross.at[k - 1, part],
                          cross_send.at[k - 1, i], cross_recv.at[k - 1, i], target)
            copy.start()
            sends.append(copy)
    factor = 0.5 * scale[...]
    for i, part in enumerate(parts):
        remote(pair.at[0, part], pair.at[0, part], pair_send.at[0, i], pair_recv.at[0, i], partner).wait_recv()
        total = partial[part, columns(tp)].astype(jnp.float32) + pair[0, part].astype(jnp.float32)
        for k in range(1, nx):
            remote(cross.at[k - 1, part], cross.at[k - 1, part], cross_send.at[k - 1, i],
                   cross_recv.at[k - 1, i], partner).wait_recv()
            total = total + cross[k - 1, part].astype(jnp.float32)
        result = (resid[part].astype(jnp.float32) + total * factor).astype(jnp.bfloat16)
        if not gathers:
            out[part] = result
            continue
        out[part, columns(tp)] = result
        gather_send, gather_recv = sems[4:]
        for k in range(1, nx):
            copy = remote(out.at[part, columns(tp)], out.at[part, columns(tp)], gather_send.at[k - 1, i], gather_recv.at[tp, i],
                          (x + k) % nx * 2 + core)
            copy.start()
            sends.append(copy)
        copy = remote(out.at[part, columns(tp)], out.at[part, columns(tp)], gather_send.at[nx - 1, i], gather_recv.at[tp, i], partner)
        copy.start()
        sends.append(copy)
    if gathers:
        for k in range(1, nx):
            slot = (x + k) % nx * 2 + core
            for i, part in enumerate(parts):
                remote(out.at[part, columns(slot)], out.at[part, columns(slot)], gather_send.at[0, i], gather_recv.at[slot, i],
                       partner).wait_recv()
                copy = remote(out.at[part, columns(slot)], out.at[part, columns(slot)], gather_send.at[nx - 1 + k, i],
                              gather_recv.at[slot, i], partner)
                copy.start()
                sends.append(copy)
        for k in range(nx):
            slot = (x + k) % nx * 2 + (1 - core)
            for i, part in enumerate(parts):
                remote(out.at[part, columns(slot)], out.at[part, columns(slot)], gather_send.at[0, i], gather_recv.at[slot, i],
                       partner).wait_recv()
    for copy in sends:
        copy.wait_send()


def summed(ntp, gathers, identity, partial, resid, scale):
    nx = ntp // 2
    rows, width = resid.shape
    pieces = 3 if rows % 48 == 0 else 1
    vmem = pl.BlockSpec(memory_space=pltpu.VMEM)
    dma = pltpu.SemaphoreType.DMA
    scratch = [
        pltpu.VMEM((nx, rows, width), jnp.bfloat16),
        pltpu.VMEM((max(nx - 1, 1), rows, width), jnp.bfloat16),
        pltpu.VMEM((max(nx - 1, 1), rows, width), jnp.bfloat16),
        dma((nx, pieces)), dma((nx, pieces)), dma((nx, pieces)), dma((nx, pieces)),
    ]
    if gathers:
        scratch += [dma((2 * nx, pieces)), dma((ntp, pieces))]
    return pl.pallas_call(
        functools.partial(sum_kernel, ntp, gathers, pieces),
        name="sum_and_share" if gathers else "sum_last",
        out_shape=jax.ShapeDtypeStruct((rows, width * (ntp if gathers else 1)), jnp.bfloat16),
        in_specs=[vmem] * 3,
        out_specs=vmem,
        scratch_shapes=scratch,
        compiler_params=pltpu.CompilerParams(
            collective_id=identity, has_side_effects=True, vmem_limit_bytes=32 << 20
        ),
    )(partial, resid, scale.reshape(1, width))


def rms(floats, norm_gain):
    scaled = floats * lax.rsqrt(jnp.mean(floats * floats, axis=-1, keepdims=True) + eps)
    return (scaled * norm_gain).astype(jnp.bfloat16)


def window_weights():
    position = jnp.arange(SEQ)
    rows, cols = position[:, None], position[None, :]
    mats = []
    for window in WINDOWS:
        low = jnp.maximum(rows - window // 2, 0)
        high = jnp.minimum(rows + window - window // 2, SEQ)
        mats.append(((cols >= low) & (cols < high)).astype(jnp.bfloat16))
    return mats


def pooling(pool_input):
    channels = pool_input.shape[1]
    group = channels // 4
    values = pool_input.reshape(-1, SEQ, channels)
    position = jnp.arange(SEQ)
    parts = []
    for index, (window, members) in enumerate(zip(WINDOWS, window_weights())):
        own = values[:, :, index * group:(index + 1) * group]
        sums = jnp.einsum("pq,sqc->spc", members, own, preferred_element_type=jnp.float32)
        before = window // 2
        counts = (
            jnp.minimum(position + window - before, SEQ) - jnp.maximum(position - before, 0)
        ).astype(jnp.float32)
        parts.append(sums / counts[None, :, None] - own.astype(jnp.float32))
    return jnp.concatenate(parts, axis=2).reshape(-1, channels).astype(jnp.bfloat16)


def body(
    nfs, ntp,
    stream, gain_first, gain_mixer, gain_second,
    gate_weight, gate_scale, up_weight, up_scale, down_weight, down_scale,
    pool_in_weight, pool_in_scale, pool_out_weight, pool_out_scale,
):
    half = jnp.bfloat16
    in_half, out_half = pool_in_weight.astype(half), pool_out_weight.astype(half)
    width, channels = stream.shape[1], in_half.shape[1]
    scales = jnp.concatenate([pool_in_scale, pool_out_scale]).reshape(1, -1)
    in_all, out_all, gate_all, up_all, down_all, stream_all, scales_all = gather_all(
        nfs, ntp, in_half, out_half, gate_weight.astype(half), up_weight.astype(half), down_weight.astype(half),
        stream, scales,
    )
    in_whole, out_whole = flat(in_all), flat(out_all)
    gate_whole, up_whole, down_whole = flat(gate_all), flat(up_all), flat(down_all)
    in_scale = scales_all[:, 0, :channels].reshape(-1)
    out_scale = scales_all[:, 0, channels:].reshape(-1)
    tp = lax.axis_index("tp")

    def feed_forward(rows):
        gate_sum = jnp.dot(rows, gate_whole, preferred_element_type=jnp.float32) * gate_scale
        up_sum = jnp.dot(rows, up_whole, preferred_element_type=jnp.float32) * up_scale
        hidden = (jax.nn.silu(gate_sum) * up_sum).astype(half)
        return jnp.dot(hidden, down_whole, preferred_element_type=jnp.float32).astype(half)

    first = rms(flat(stream_all).astype(jnp.float32), gain_first)
    after_first = summed(ntp, True, 1, feed_forward(first), stream, down_scale)
    mixer_normed = rms(after_first.astype(jnp.float32), gain_mixer)
    pool_input = (
        jnp.dot(mixer_normed, in_whole, preferred_element_type=jnp.float32) * in_scale
    ).astype(half)
    mixed = jnp.dot(pooling(pool_input), out_whole, preferred_element_type=jnp.float32)
    after_mix = (after_first.astype(jnp.float32) + mixed * out_scale).astype(half)
    second = rms(after_mix.astype(jnp.float32), gain_second)
    own = lax.dynamic_slice_in_dim(after_mix, tp * stream.shape[1], stream.shape[1], axis=1)
    return summed(ntp, False, 2, feed_forward(second), own, down_scale)


def solution(mesh):
    placed = (
        P("fs", "tp"), P(), P(), P(),
        P("fs", "tp"), P("tp"), P("fs", "tp"), P("tp"), P("tp", "fs"), P("tp"),
        P("fs", "tp"), P("tp"), P("tp", "fs"), P("tp"),
    )
    return jax.shard_map(
        functools.partial(body, mesh.shape["fs"], mesh.shape["tp"]),
        mesh=mesh, in_specs=placed, out_specs=P("fs", "tp"), check_vma=False,
    )
```

profile of v0, /device:TPU:0, one launch (start us, length us, event | category | flops | bytes accessed | tf_op | source)
XLA Modules:
  0.0 271.6 jit_solution(12734682890409593270)
XLA Ops:
  0.0 1.6 convert_element_type.102.gate
  1.6 0.2 copy-done.8
  1.8 0.0 copy-start
  1.8 0.1 convert_element_type.103.up
  1.9 0.3 copy-done.9
  2.2 0.1 convert_element_type.104.down
  2.3 0.5 copy-done.10
  2.8 0.0 copy-done.11
  2.9 0.0 copy-done.13
  2.9 0.0 copy-done.15
  2.9 0.0 copy-start.16
  2.9 0.0 copy-start.18
  2.9 0.1 copy-done
  3.0 184.7 %collect_weights.1 = (bf16[2048,512]{1,0:T(8,128)(2,1)S(1)}, bf16[512,2048]{1,0:T(8,128)(2,1)S(1)}, bf16[2048,1408]{1,0:T(8,128)(2,1)S(1)}, bf16[2048,1408]{1,0:...) custom-call(bf16[256,128]{1,0:T(8,128)(2,1)S(1)} %convert_element_type.10, ...), custom_call_target="tpu_custom_call" | custom-call | tf_op jit(solution)/shard_map/collect_weights/pallas_call | solution.py:284
  187.7 0.0 copy-start.2
  187.8 2.5 copy-done.2
  190.3 2.5 copy-done.3
  192.8 1.3 copy-done.5
  194.1 1.4 copy-done.6
  195.5 0.4 fusion
  195.9 0.0 copy-done.16
  195.9 0.0 copy-done.18
  195.9 4.1 %convolution_multiply_fusion.3 = f32[384,1408]{1,0:T(8,128)} fusion(bf16[2048,1408]{1,0:T(8,128)(2,1)S(1)} %get-tuple-element.13, f32[1408]{0:T(1024)S(1)} %copy-done.18, bf16[384,2048]{1,0:T(8,128)(2,1)S(1)} %get-tuple-element.12, f32[2048]{0:T(1024)S(1)} %copy-done.16, f32[384]{0:T(512)S(1)} %add_rsqrt_fusion.2), kind=kOutput, calls=%fused_computation.22 | convolution fusion | flops 2218278912 | bytes 9518080 | tf_op jit(solution)/shard_map/dot_general | solution.py:472
  200.0 0.0 copy-done.4
  200.0 10.1 %convolution_convert_fusion.1.partial = bf16[384,2048]{1,0:T(8,128)(2,1)S(1)} fusion(bf16[1408,2048]{1,0:T(8,128)(2,1)} %copy-done.3, bf16[2048,1408]{1,0:T(8,128)(2,1)} %copy-done.2, f32[384,1408]{1,0:T(8,128)} %convolution_multiply_fusion.3, f32[1408]{0:T(1024)} %param.21, bf16[384,2048]{1,0:T(8,128)(2,1)S(1)} %get-tuple-element.12, f32[2048]{0:T(1024)} %param.15, ...), kind=kOutput, calls=%fused_computation.24 | convolution fusion | flops 4436901888 | bytes 16858112 | tf_op jit(solution)/shard_map/dot_general | solution.py:475
  210.1 0.0 copy-start.17
  210.1 21.7 %sum_and_share.1 = bf16[384,2048]{1,0:T(8,128)(2,1)S(1)} custom-call(bf16[384,2048]{1,0:T(8,128)(2,1)S(1)} %convolution_convert_fusion.1.partial, bf16[384,512]{1,0:T(8,128)(2,1)S(1)} %copy-done, f32[1,512]{1,0:T(1,128)S(1)} %bitcast.50), custom_call_target="tpu_custom_call" | custom-call | tf_op jit(solution)/shard_map/sum_and_share/pallas_call | solution.py:405
  231.9 0.4 fusion.6
  232.3 1.0 fusion.21
  233.3 0.1 fusion.68
  233.4 0.1 copy.24
  233.6 0.3 fusion.32
  233.8 0.1 copy.25
  234.0 0.3 fusion.33
  234.3 0.1 copy.26
  234.4 0.3 fusion.34
  234.7 0.1 copy.27
  234.8 0.3 fusion.35
  235.2 0.2 copy.23
  235.3 0.0 copy-start.19
  235.4 0.0 copy-start.21
  235.4 2.8 %fusion.3 = (f32[384]{0:T(512)S(1)}, bf16[384,2048]{1,0:T(8,128)(2,1)S(1)}) fusion(f32[2048]{0:T(1024)S(1)} %bitcast.58, bf16[384,512]{1,0:T(8,128)(2,1)S(1)} %bitcast.57, bf16[512,2048]{1,0:T(8,128)(2,1)} %copy-done.5, bf16[384,2048]{1,0:T(8,128)(2,1)S(1)} %sum_and_share.1), kind=kOutput, calls=%fused_computation.10 | convolution fusion | flops 810811008 | bytes 5645824 | tf_op jit(solution)/shard_map/dot_general | solution.py:483
  238.2 1.1 copy-done.12
  239.4 6.9 %convolution_multiply_fusion.1 = f32[384,1408]{1,0:T(8,128)} fusion(bf16[2048,1408]{1,0:T(8,128)(2,1)} %copy-done.4, f32[1408]{0:T(1024)S(1)} %copy-done.19, bf16[384,2048]{1,0:T(8,128)(2,1)S(1)} %get-tuple-element.24, f32[2048]{0:T(1024)S(1)} %copy-done.21, f32[384]{0:T(512)S(1)} %add_rsqrt_fusion), kind=kOutput, calls=%fused_computation.19 | convolution fusion | flops 2218278912 | bytes 9518080 | tf_op jit(solution)/shard_map/dot_general | solution.py:472
  246.3 10.5 %convolution_convert_fusion.partial = bf16[384,2048]{1,0:T(8,128)(2,1)S(1)} fusion(bf16[1408,2048]{1,0:T(8,128)(2,1)} %copy-done.3, bf16[2048,1408]{1,0:T(8,128)(2,1)} %copy-done.2, f32[384,1408]{1,0:T(8,128)} %convolution_multiply_fusion.1, f32[1408]{0:T(1024)S(1)} %copy-done.20, bf16[384,2048]{1,0:T(8,128)(2,1)} %copy-done.12, f32[2048]{0:T(1024)S(1)} %copy-done.21, ...), kind=kOutput, calls=%fused_computation.23 | convolution fusion | flops 4436901888 | bytes 16858112 | tf_op jit(solution)/shard_map/dot_general | solution.py:475
  256.8 1.0 constant_dynamic-slice_fusion.resid
  257.8 13.0 %sum_last.1 = bf16[384,512]{1,0:T(8,128)(2,1)S(1)} custom-call(bf16[384,2048]{1,0:T(8,128)(2,1)S(1)} %convolution_convert_fusion.partial, bf16[384,512]{1,0:T(8,128)(2,1)S(1)} %constant_dynamic-slice_fusion.resid, f32[1,512]{1,0:T(1,128)S(1)} %bitcast.51), custom_call_target="tpu_custom_call" | custom-call | tf_op jit(solution)/shard_map/sum_last/pallas_call | solution.py:405
  270.8 0.7 copy.29
  (40 shorter events, 0.2 us)
Async XLA Ops:
  0.0 1.8 copy-start.8
  0.0 2.2 copy-start.9
  1.8 1.0 copy-start.10
  1.8 1.0 copy-start.11
  1.8 1.1 copy-start.13
  1.8 1.1 copy-start.15
  1.8 1.2 copy-start
  2.9 193.0 %copy-start.16 = (f32[2048]{0:T(1024)S(1)}, f32[2048]{0:T(1024)}, u32[]{:S(2)}) copy-start(f32[2048]{0:T(1024)} %param.15) | copy-start | bytes 24580
  2.9 193.0 %copy-start.18 = (f32[1408]{0:T(1024)S(1)}, f32[1408]{0:T(1024)}, u32[]{:S(2)}) copy-start(f32[1408]{0:T(1024)} %param.19) | copy-start | bytes 16900
  187.7 2.5 copy-start.2
  190.3 2.5 copy-start.3
  192.8 1.4 copy-start.5
  194.1 1.4 copy-start.6
  195.5 4.5 %copy-start.4 = (bf16[2048,1408]{1,0:T(8,128)(2,1)}, bf16[2048,1408]{1,0:T(8,128)(2,1)S(1)}, u32[]{:S(2)}) copy-start(bf16[2048,1408]{1,0:T(8,128)(2,1)S(1)} %get-tuple-element.13) | copy-start | bytes 17301508
  195.9 4.1 %copy-start.14 = (f32[384]{0:T(512)}, f32[384]{0:T(512)S(1)}, u32[]{:S(2)}) copy-start(f32[384]{0:T(512)S(1)} %add_rsqrt_fusion.2) | copy-start | bytes 4612
  200.0 10.1 %copy-start.1 = (f32[512]{0:T(512)S(1)}, f32[512]{0:T(512)}, u32[]{:S(2)}) copy-start(f32[512]{0:T(512)} %param.23) | copy-start | bytes 6148
  210.1 22.2 %copy-start.7 = (bf16[2048,512]{1,0:T(8,128)(2,1)S(1)}, bf16[2048,512]{1,0:T(8,128)(2,1)}, u32[]{:S(2)}) copy-start(bf16[2048,512]{1,0:T(8,128)(2,1)} %copy-done.6) | copy-start | bytes 6291460
  210.1 22.2 %copy-start.17 = (f32[2048]{0:T(1024)S(1)}, f32[2048]{0:T(1024)}, u32[]{:S(2)}) copy-start(f32[2048]{0:T(1024)} %param.16) | copy-start | bytes 24580
  235.3 4.0 %copy-start.19 = (f32[1408]{0:T(1024)S(1)}, f32[1408]{0:T(1024)}, u32[]{:S(2)}) copy-start(f32[1408]{0:T(1024)} %param.19) | copy-start | bytes 16900
  235.4 4.0 %copy-start.21 = (f32[2048]{0:T(1024)S(1)}, f32[2048]{0:T(1024)}, u32[]{:S(2)}) copy-start(f32[2048]{0:T(1024)} %param.17) | copy-start | bytes 24580
  238.2 1.2 copy-start.12
  239.4 6.9 %copy-start.20 = (f32[1408]{0:T(1024)S(1)}, f32[1408]{0:T(1024)}, u32[]{:S(2)}) copy-start(f32[1408]{0:T(1024)} %param.21) | copy-start | bytes 16900
where the time goes:
time: 272 us
  Pallas kernels  219 us (81%)
  matrix products  36.5 us (13%)
  local copies, waits for them, and re-layouts  12.6 us (5%)
    pallas_call x1, Pallas kernels, gather_all(): pl.pallas_call(functools.partial(gather_kernel, nfs, ntp), name='collect_...  185 us
    pallas_call x2, Pallas kernels, summed(): pl.pallas_call(functools.partial(sum_kernel, ntp, gathers, pieces), name=...  34.7 us
    dot_general x2, matrix products, feed_forward(): jnp.dot(hidden, down_whole, preferred_element_type=jnp.float32).astype(half)  20.6 us
    unnamed x50, local copies, waits for them, and re-layouts  11.4 us
    dot_general x2, matrix products, feed_forward(): jnp.dot(rows, gate_whole, preferred_element_type=jnp.float32) * gate_scale  10.9 us

commit v1 on v0

--- a/solution.py
+++ b/solution.py
@@ -448,6 +448,468 @@
     return jnp.concatenate(parts, axis=2).reshape(-1, channels).astype(jnp.bfloat16)
 
 
+def layer_kernel(
+    sizes, stream, gate, up, down, pool_in, pool_out, scales, gains, gate_scale, up_scale, down_scale, out,
+    gate_all, up_all, down_all, in_all, out_all, scales_all, rows_all, first_all, mixed_all, normed,
+    gate_sum, up_sum, hidden, pooled, partial, pair, shares,
+    local_sem, z_send, y_send, w_recv, pl_zsend, pl_ysend, pl_recv, slab_send, slab_recv,
+    sc_send, sc_recv, ag_send, ag_recv, pair_send, pair_recv, rs_send, rs_recv,
+):
+    rows, small, extra = sizes
+    big = small + extra
+    block = gate.shape[0]
+    width = stream.shape[1]
+    chans = pool_in.shape[1]
+    features = gate_all.shape[0]
+    every = 2 * rows
+    f32, half = jnp.float32, jnp.bfloat16
+    fs, tp = lax.axis_index("fs"), lax.axis_index("tp")
+    z, y = fs // 2, fs % 2
+    x, core = tp // 2, tp % 2
+    low, pair_hi = z % 2, z // 2
+    zp = z + 1 - 2 * low
+    zs = [z, zp, 2 - pair_hi, 3 - 3 * pair_hi]
+    fs_y, fs_z = fs + 1 - 2 * y, 2 * zp + y
+    tp_c, tp_x = tp + 1 - 2 * core, (tp + 2) % 4
+    tp_xc = tp_x + 1 - 2 * core
+
+    def upper(at):
+        return (((at + 1) // 2) % 2 + core) % 2
+
+    barrier = pltpu.get_barrier_semaphore()
+    peers = [(2 * at + y, tp) for at in zs[1:]] + [
+        (fs_y, tp), (fs, tp_c), (fs, tp_x), (fs, tp_xc), (fs_z, tp_x)]
+    for f, t in peers:
+        pl.semaphore_signal(barrier, inc=1, device_id={"fs": f, "tp": t}, device_id_type=MESH)
+    pl.semaphore_wait(barrier, len(peers))
+
+    ends = []
+
+    def remote(src, dst, send, recv, f, t):
+        return pltpu.make_async_remote_copy(
+            src_ref=src, dst_ref=dst, send_sem=send, recv_sem=recv,
+            device_id={"fs": f, "tp": t}, device_id_type=MESH)
+
+    def start(make, cond=None):
+        if cond is None:
+            make().start()
+        else:
+            pl.when(cond)(lambda: make().start())
+        ends.append((make, cond))
+
+    def arrive(dst, recv, cond=None):
+        def wait():
+            remote(dst, dst, recv, recv, fs, tp_c).wait_recv()
+        if cond is None:
+            wait()
+        else:
+            pl.when(cond)(wait)
+
+    def lanes(at, count):
+        return pl.ds(pl.multiple_of(at, 128), count)
+
+    def subs(at, count):
+        return pl.ds(pl.multiple_of(at, 16), count)
+
+    own_rows = subs(low * rows, rows)
+
+    def share_place(ref, chip_low, t, j):
+        return ref.at[subs(chip_low * rows, rows), lanes(t * width + j * block, block)]
+
+    def share_start(phase, ref, j, src):
+        dst = share_place(ref, low, tp, j)
+        chip = 2 * x + low
+        for k, (f, t) in enumerate(((fs_z, tp), (fs, tp_x), (fs_z, tp_x), (fs, tp_c))):
+            start(lambda f=f, t=t, k=k: remote(
+                src, dst, ag_send.at[phase, j, k], ag_recv.at[phase, j, chip, core], f, t))
+
+    def share_forward(phase, ref):
+        for j in range(width // block):
+            for k, (cl, t) in enumerate(((1 - low, tp), (low, tp_x), (1 - low, tp_x))):
+                here = share_place(ref, cl, t, j)
+                chip = 2 * (t // 2) + cl
+                arrive(here, ag_recv.at[phase, j, chip, core])
+                start(lambda here=here, chip=chip, k=k, j=j: remote(
+                    here, here, ag_send.at[phase, j, 4 + k], ag_recv.at[phase, j, chip, core], fs, tp_c))
+
+    def share_finish(phase, ref):
+        for j in range(width // block):
+            for cl, t in ((low, tp_c), (1 - low, tp_c), (low, tp_xc), (1 - low, tp_xc)):
+                arrive(share_place(ref, cl, t, j), ag_recv.at[phase, j, 2 * (t // 2) + cl, 1 - core])
+
+    stream_own = pltpu.make_async_copy(
+        stream, rows_all.at[own_rows, lanes(tp * width, width)], local_sem.at[0])
+    stream_own.start()
+    for j in range(width // block):
+        share_start(0, rows_all, j, stream.at[:, j * block:(j + 1) * block])
+
+    def scale_copy(k, slot, t):
+        return remote(scales, scales_all.at[slot], sc_send.at[k], sc_recv.at[slot], fs, t)
+
+    for k, t in enumerate((tp_c, tp_x, tp_xc)):
+        start(lambda k=k, t=t: scale_copy(k, tp, t))
+    locals_ = [pltpu.make_async_copy(scales, scales_all.at[tp], local_sem.at[1])]
+
+    def pool_place(which, f, t):
+        if which == 0:
+            return in_all.at[subs(f * block, block), lanes(t * chans, chans)]
+        return out_all.at[subs(t * chans, chans), lanes(f * block, block)]
+
+    def pool_slab(which, t):
+        if which == 0:
+            return in_all.at[:, lanes(t * chans, chans)]
+        return out_all.at[subs(t * chans, chans)]
+
+    for which, own in enumerate((pool_in, pool_out)):
+        locals_.append(pltpu.make_async_copy(own, pool_place(which, fs, tp), local_sem.at[2 + which]))
+        for k in range(1, 4):
+            start(lambda k=k, which=which, own=own: remote(
+                own, pool_place(which, fs, tp), pl_zsend.at[which, k], pl_recv.at[which, fs], 2 * zs[4 - k] + y, tp))
+        start(lambda which=which, own=own: remote(
+            own, pool_place(which, fs, tp), pl_ysend.at[which, 0], pl_recv.at[which, fs], fs_y, tp))
+
+    def own_part(piece, part, side):
+        first, count = (side * small, small) if part == 0 else (2 * small, extra)
+        ref = (gate, up, down)[piece]
+        return ref.at[subs(first, count)] if piece == 2 else ref.at[:, lanes(first, count)]
+
+    def all_part(piece, part, f):
+        first, count = (0, small) if part == 0 else (small, extra)
+        if piece == 2:
+            return down_all.at[f, pl.ds(first, count)]
+        return (gate_all, up_all)[piece].at[subs(f * block, block), pl.ds(first, count)]
+
+    def y_own(piece):
+        for part in range(2):
+            start(lambda part=part: remote(
+                own_part(piece, part, upper(z)), all_part(piece, part, fs), y_send.at[0, piece, part],
+                w_recv.at[fs, piece, part], fs_y, tp), None if part == 0 else upper(z) == 1)
+
+    def own_copy(piece, part):
+        return pltpu.make_async_copy(
+            own_part(piece, part, upper(z)), all_part(piece, part, fs), local_sem.at[4 + 2 * piece + part])
+
+    for copy in locals_:
+        copy.start()
+    for piece in range(3):
+        for k in (3, 2, 1):
+            at = zs[k]
+            for part in range(2):
+                start(lambda k=k, at=at, part=part, piece=piece: remote(
+                    own_part(piece, part, upper(at)), all_part(piece, part, fs), z_send.at[k, piece, part],
+                    w_recv.at[fs, piece, part], 2 * at + y, tp), None if part == 0 else upper(at) == 1)
+        if piece < 2:
+            y_own(piece)
+        own_copy(piece, 0).start()
+        pl.when(upper(z) == 1)(lambda piece=piece: own_copy(piece, 1).start())
+
+    @pl.when(upper(z) == 0)
+    def _():
+        gate_all[:, small:big] = jnp.zeros((features, extra), half)
+        up_all[:, small:big] = jnp.zeros((features, extra), half)
+        down_all[:, small:big, :] = jnp.zeros((down_all.shape[0], extra, block), half)
+
+    def weights_here(piece, f):
+        arrive(all_part(piece, 0, f), w_recv.at[f, piece, 0])
+        arrive(all_part(piece, 1, f), w_recv.at[f, piece, 1], upper(z) == 1)
+
+    def by_z(piece, i):
+        f = 2 * zs[i] + y
+        weights_here(piece, f)
+        for part in range(2):
+            start(lambda part=part: remote(
+                all_part(piece, part, f), all_part(piece, part, f), y_send.at[i, piece, part],
+                w_recv.at[f, piece, part], fs_y, tp), None if part == 0 else upper(z) == 1)
+
+    def own_here(piece):
+        own_copy(piece, 0).wait()
+        pl.when(upper(z) == 1)(lambda: own_copy(piece, 1).wait())
+
+    step = 32
+
+    def norm_rows(source, gain_row):
+        def one(i, carry):
+            part = pl.ds(pl.multiple_of(i * step, step), step)
+            floats = source[part, :].astype(f32)
+            scale = lax.rsqrt(jnp.mean(floats * floats, axis=-1, keepdims=True) + eps)
+            normed[part, :] = ((floats * scale) * gains[gain_row:gain_row + 1, :]).astype(half)
+            return carry
+        return one
+
+    stream_own.wait()
+    share_forward(0, rows_all)
+    share_finish(0, rows_all)
+    lax.fori_loop(0, every // step, norm_rows(rows_all, 0), 0)
+
+    for k in range(1, 4):
+        for which in range(2):
+            f = 2 * zs[k] + y
+            here = pool_place(which, f, tp)
+            arrive(here, pl_recv.at[which, f])
+            start(lambda k=k, which=which, here=here, f=f: remote(
+                here, here, pl_ysend.at[which, k], pl_recv.at[which, f], fs_y, tp))
+
+    tile = 256
+
+    def accumulate(weights, total, f, first):
+        def one(i, carry):
+            part = pl.ds(pl.multiple_of(i * tile, tile), tile)
+            product = jnp.dot(normed[part, lanes(f * block, block)], weights[subs(f * block, block), :],
+                              preferred_element_type=f32)
+            total[part, :] = product if first else total[part, :] + product
+            return carry
+        lax.fori_loop(0, every // tile, one, 0)
+
+    for i in range(4):
+        f, g = 2 * zs[i] + y, 2 * zs[i] + 1 - y
+        for piece, (weights, total) in enumerate(((gate_all, gate_sum), (up_all, up_sum))):
+            if i == 0:
+                own_here(piece)
+            accumulate(weights, total, f, i == 0)
+        if i < 3:
+            by_z(0, i + 1)
+            by_z(1, i + 1)
+        else:
+            y_own(2)
+            own_here(2)
+        for piece, (weights, total) in enumerate(((gate_all, gate_sum), (up_all, up_sum))):
+            weights_here(piece, g)
+            accumulate(weights, total, g, False)
+        if i == 1:
+            for which in range(2):
+                locals_[1 + which].wait()
+                for k in range(4):
+                    if k:
+                        arrive(pool_place(which, 2 * zs[k] + 1 - y, tp), pl_recv.at[which, 2 * zs[k] + 1 - y])
+                    else:
+                        arrive(pool_place(which, fs_y, tp), pl_recv.at[which, fs_y])
+                slab = pool_slab(which, tp)
+                start(lambda which=which, slab=slab: remote(
+                    slab, slab, slab_send.at[which, 0], slab_recv.at[which, tp], fs, tp_x))
+                start(lambda which=which, slab=slab: remote(
+                    slab, slab, slab_send.at[which, 1], slab_recv.at[which, tp], fs, tp_c))
+
+    side = lanes(upper(z) * small, big)
+
+    def hide(i, carry):
+        part = pl.ds(pl.multiple_of(i * step, step), step)
+        a = gate_sum[part, :] * gate_scale[:, side]
+        hidden[part, :] = (a / (1.0 + jnp.exp(-a)) * (up_sum[part, :] * up_scale[:, side])).astype(half)
+        return carry
+
+    lax.fori_loop(0, every // step, hide, 0)
+
+    def block_product(phase, f):
+        def one(i, carry):
+            part = pl.ds(pl.multiple_of(i * tile, tile), tile)
+            partial[phase, f, part, :] = jnp.dot(
+                hidden[part, :], down_all[f], preferred_element_type=f32).astype(half)
+            return carry
+        lax.fori_loop(0, every // tile, one, 0)
+        zz = f // 2
+        slot = 2 * (zz // 2) + f % 2
+        start(lambda: remote(
+            partial.at[phase, f], pair.at[phase, slot], pair_send.at[phase, f], pair_recv.at[phase, slot], fs, tp_c),
+            zz % 2 != core)
+
+    def block_sum(phase, f):
+        zz = f // 2
+        slot = 2 * (zz // 2) + f % 2
+        here, there = subs(low * rows, rows), subs((1 - low) * rows, rows)
+
+        @pl.when(zz % 2 == core)
+        def _():
+            remote(pair.at[phase, slot], pair.at[phase, slot], pair_send.at[phase, f], pair_recv.at[phase, slot],
+                   fs, tp_c).wait_recv()
+
+            def one(i, carry):
+                part = pl.ds(pl.multiple_of(i * 128, 128), 128)
+                partial[phase, f, part, :] = (
+                    partial[phase, f, part, :].astype(f32) + pair[phase, slot, part, :].astype(f32)).astype(half)
+                return carry
+            lax.fori_loop(0, every // 128, one, 0)
+
+        mine = zz // 2 == x
+        for k, (part, fd, td, cond) in enumerate((
+            (here, fs, tp_x, jnp.logical_not(mine)), (there, fs_z, tp, mine), (there, fs_z, tp_x, jnp.logical_not(mine)),
+        )):
+            start(lambda k=k, part=part, fd=fd, td=td: remote(
+                partial.at[phase, f, part], shares.at[phase, k, f % 2], rs_send.at[phase, slot, k],
+                rs_recv.at[phase, k, f % 2], fd, td), (zz % 2 == core) & cond)
+
+    def block_total(phase, j, resid, target):
+        f = 2 * tp + j
+        for k in range(3):
+            arrive(shares.at[phase, k, j], rs_recv.at[phase, k, j])
+
+        def one(i, carry):
+            at = pl.multiple_of(i * 64, 64)
+            total = partial[phase, f, pl.ds(pl.multiple_of(low * rows + at, 64), 64), :].astype(f32)
+            for k in range(3):
+                total = total + shares[phase, k, j, pl.ds(at, 64), :].astype(f32)
+            cols = slice(j * block, (j + 1) * block)
+            target(at, j, (resid(at, j) + total * (0.5 * down_scale[:, cols])).astype(half))
+            return carry
+        lax.fori_loop(0, rows // 64, one, 0)
+
+    def stream_part(at, j):
+        return stream[pl.ds(at, 64), j * block:(j + 1) * block].astype(f32)
+
+    def first_part(at, j, value):
+        first_all[pl.ds(pl.multiple_of(low * rows + at, 64), 64), lanes(tp * width + j * block, block)] = value
+
+    def first_done(i):
+        @pl.when(zs[i] == tp)
+        def _():
+            for j in range(2):
+                block_total(0, j, stream_part, first_part)
+
+    by_z(2, 1)
+    for i in range(4):
+        f, g = 2 * zs[i] + y, 2 * zs[i] + 1 - y
+        block_product(0, f)
+        block_sum(0, f)
+        if 1 <= i < 3:
+            by_z(2, i + 1)
+        if i == 1:
+            for which in range(2):
+                slab = pool_slab(which, tp_x)
+                arrive(slab, slab_recv.at[which, tp_x])
+                start(lambda which=which, slab=slab: remote(
+                    slab, slab, slab_send.at[which, 2], slab_recv.at[which, tp_x], fs, tp_c))
+        weights_here(2, g)
+        block_product(0, g)
+        block_sum(0, g)
+        if i == 2:
+            first_done(0)
+            first_done(1)
+        if i == 3:
+            first_done(2)
+            first_done(3)
+    for j in range(2):
+        share_start(1, first_all, j, share_place(first_all, low, tp, j))
+    for which in range(2):
+        for t in (tp_c, tp_xc):
+            arrive(pool_slab(which, t), slab_recv.at[which, t])
+    locals_[0].wait()
+    for t in (tp_c, tp_x, tp_xc):
+        arrive(scales_all.at[t], sc_recv.at[t])
+    share_forward(1, first_all)
+    share_finish(1, first_all)
+
+    in_scale = jnp.concatenate([scales_all[t, :, :chans] for t in range(4)], axis=1)
+    lax.fori_loop(0, every // step, norm_rows(first_all, 1), 0)
+    group = 4 * chans // 4
+    pos_row = lax.broadcasted_iota(jnp.int32, (SEQ, SEQ), 0)
+    pos_col = lax.broadcasted_iota(jnp.int32, (SEQ, SEQ), 1)
+    pos = lax.broadcasted_iota(jnp.int32, (SEQ, 1), 0)
+
+    def mix(h, carry):
+        base = pl.multiple_of(h * rows, rows)
+        part = pl.ds(base, rows)
+        pool_input = (jnp.dot(normed[part, :], in_all[...], preferred_element_type=f32) * in_scale).astype(half)
+        for index, window in enumerate(WINDOWS):
+            before = window // 2
+            first = jnp.maximum(pos_row - before, 0)
+            last = jnp.minimum(pos_row + window - before, SEQ)
+            members = jnp.where((pos_col >= first) & (pos_col < last), 1.0, 0.0).astype(half)
+            counts = (jnp.minimum(pos + window - before, SEQ) - jnp.maximum(pos - before, 0)).astype(f32)
+            for s in range(rows // SEQ):
+                own = pool_input[s * SEQ:(s + 1) * SEQ, index * group:(index + 1) * group]
+                sums = jnp.dot(members, own, preferred_element_type=f32)
+                pooled[s * SEQ:(s + 1) * SEQ, index * group:(index + 1) * group] = (
+                    sums / counts - own.astype(f32)).astype(half)
+        for t in range(4):
+            cols = slice(t * width, (t + 1) * width)
+            mixed = jnp.dot(pooled[...], out_all[:, cols], preferred_element_type=f32)
+            mixed_all[part, cols] = (
+                first_all[part, cols].astype(f32) + mixed * scales_all[t, :, chans:]).astype(half)
+        return carry
+
+    lax.fori_loop(0, 2, mix, 0)
+    lax.fori_loop(0, every // step, norm_rows(mixed_all, 2), 0)
+
+    def both(i, carry):
+        part = pl.ds(pl.multiple_of(i * tile, tile), tile)
+        a = jnp.dot(normed[part, :], gate_all[...], preferred_element_type=f32) * gate_scale[:, side]
+        b = jnp.dot(normed[part, :], up_all[...], preferred_element_type=f32) * up_scale[:, side]
+        hidden[part, :] = (a / (1.0 + jnp.exp(-a)) * b).astype(half)
+        return carry
+
+    lax.fori_loop(0, every // tile, both, 0)
+    order = [2 * zz + j for zz in (2 * (1 - x), 2 * (1 - x) + 1, 2 * x, 2 * x + 1) for j in range(2)]
+    for k, f in enumerate(order):
+        block_product(1, f)
+        if k:
+            block_sum(1, order[k - 1])
+    block_sum(1, order[-1])
+
+    def mixed_part(at, j):
+        return mixed_all[pl.ds(pl.multiple_of(low * rows + at, 64), 64), lanes(tp * width + j * block, block)].astype(f32)
+
+    def out_part(at, j, value):
+        out[pl.ds(at, 64), j * block:(j + 1) * block] = value
+
+    for j in range(2):
+        block_total(1, j, mixed_part, out_part)
+
+    for make, cond in ends:
+        if cond is None:
+            make().wait_send()
+        else:
+            pl.when(cond)(lambda make=make: make().wait_send())
+
+
+def fits(nfs, ntp, stream, gate, pool_in):
+    ny, nz = fs_grid(nfs)
+    tiles = gate.shape[1] // 128
+    return (
+        (ny, nz, ntp) == (2, 4, 4) and gate.shape[1] % 128 == 0 and tiles % 2 == 1 and tiles > 1
+        and stream.shape[0] % SEQ == 0 and stream.shape[0] % 128 == 0 and pool_in.shape[1] % 128 == 0
+        and gate.shape[0] % 128 == 0 and stream.shape[1] == 2 * gate.shape[0]
+        and 2 * stream.shape[0] % 256 == 0
+    )
+
+
+def whole_layer(stream, gains, gate, gate_scale, up, up_scale, down, down_scale, pool_in, pool_out, scales):
+    rows, width = stream.shape
+    block, units = gate.shape
+    chans = pool_in.shape[1]
+    features = 4 * width
+    small = (units // 128 // 2) * 128
+    extra = units - 2 * small
+    big = small + extra
+    every = 2 * rows
+    f32, half = jnp.float32, jnp.bfloat16
+    vmem = pl.BlockSpec(memory_space=pltpu.VMEM)
+    dma = pltpu.SemaphoreType.DMA
+    return pl.pallas_call(
+        functools.partial(layer_kernel, (rows, small, extra)),
+        name="whole_layer",
+        out_shape=jax.ShapeDtypeStruct((rows, width), half),
+        in_specs=[vmem] * 11,
+        out_specs=vmem,
+        scratch_shapes=[
+            pltpu.VMEM((features, big), half), pltpu.VMEM((features, big), half), pltpu.VMEM((8, big, block), half),
+            pltpu.VMEM((features, 4 * chans), half), pltpu.VMEM((4 * chans, features), half),
+            pltpu.VMEM((4,) + scales.shape, f32),
+            pltpu.VMEM((every, features), half), pltpu.VMEM((every, features), half),
+            pltpu.VMEM((every, features), half), pltpu.VMEM((every, features), half),
+            pltpu.VMEM((every, big), f32), pltpu.VMEM((every, big), f32), pltpu.VMEM((every, big), half),
+            pltpu.VMEM((rows, 4 * chans), half),
+            pltpu.VMEM((2, 8, every, block), half), pltpu.VMEM((2, 4, every, block), half),
+            pltpu.VMEM((2, 3, 2, rows, block), half),
+            dma((10,)), dma((4, 3, 2)), dma((4, 3, 2)), dma((8, 3, 2)),
+            dma((2, 4)), dma((2, 4)), dma((2, 8)), dma((2, 3)), dma((2, 4)),
+            dma((3,)), dma((4,)), dma((2, 2, 7)), dma((2, 2, 4, 2)),
+            dma((2, 8)), dma((2, 4)), dma((2, 4, 3)), dma((2, 3, 2)),
+        ],
+        compiler_params=pltpu.CompilerParams(
+            collective_id=0, has_side_effects=True, vmem_limit_bytes=58 << 20),
+    )(stream, gate, up, down, pool_in, pool_out, scales, gains, gate_scale.reshape(1, -1), up_scale.reshape(1, -1),
+      down_scale.reshape(1, -1))
+
+
 def body(
     nfs, ntp,
     stream, gain_first, gain_mixer, gain_second,
@@ -458,6 +920,10 @@
     in_half, out_half = pool_in_weight.astype(half), pool_out_weight.astype(half)
     width, channels = stream.shape[1], in_half.shape[1]
     scales = jnp.concatenate([pool_in_scale, pool_out_scale]).reshape(1, -1)
+    if fits(nfs, ntp, stream, gate_weight, pool_in_weight):
+        return whole_layer(
+            stream, jnp.stack([gain_first, gain_mixer, gain_second]), gate_weight.astype(half), gate_scale,
+            up_weight.astype(half), up_scale, down_weight.astype(half), down_scale, in_half, out_half, scales)
     in_all, out_all, gate_all, up_all, down_all, stream_all, scales_all = gather_all(
         nfs, ntp, in_half, out_half, gate_weight.astype(half), up_weight.astype(half), down_weight.astype(half),
         stream, scales,

time: 272 us -> 241 us (0.89)
  matrix products: 36.5 us -> 0 us
  local copies, waits for them, and re-layouts: 12.6 us -> 5.64 us
  other arithmetic: 2.63 us -> 9.42 us
  Pallas kernels: 219 us -> 224 us
    dot_general x10 -> x0, matrix products: 36.5 us -> none  [the longest x2 20.6 us: feed_forward(): jnp.dot(hidden, down_whole, preferred_element_type=jnp.float32).astype(half)]
    unnamed x50 -> x5, local copies, waits for them, and re-layouts: 11.4 us -> 2.45 us
    pallas_call x3 -> x1, Pallas kernels: 219 us -> 224 us  [whole_layer(): pl.pallas_call(functools.partial(layer_kernel, (rows, small, extra)), nam...]
where the time goes in v1:
time: 241 us; the launch traced here: 239 us
  Pallas kernels  224 us (93%)
  other arithmetic  9.42 us (4%)
  local copies, waits for them, and re-layouts  5.64 us (2%)
    pallas_call x1, Pallas kernels, whole_layer(): pl.pallas_call(functools.partial(layer_kernel, (rows, small, extra)), nam...  224 us

profile of v1, /device:TPU:0, one launch (start us, length us, event | category | flops | bytes accessed | tf_op | source)
XLA Modules:
  0.0 238.6 jit_solution(13392764691306007853)
XLA Ops:
  0.0 0.0 copy-start
  0.0 0.8 pad_maximum_fusion.1
  0.8 0.6 reshape.12.scales
  1.4 1.3 reshape.13.gate_scale
  2.7 1.3 reshape.14.up_scale
  4.0 1.4 pad_maximum_fusion.gains
  5.4 1.5 convert_element_type.18.pool_in
  6.9 1.5 convert_element_type.19.pool_out
  8.4 2.3 convert_element_type.15.gate
  10.7 0.0 copy-done
  10.7 0.0 copy-start.1
  10.7 0.9 convert_element_type.16.up
  11.7 0.7 copy-done.1
  12.3 0.9 convert_element_type.17.down
  13.3 223.5 %whole_layer.1 = bf16[384,512]{1,0:T(8,128)(2,1)} custom-call(bf16[384,512]{1,0:T(8,128)(2,1)} %stream.1, bf16[256,1408]{1,0:T(8,128)(2,1)} %convert_element_type.15.gate, bf16[256,1408]{1,0:T(8,128)(2,1)} %convert_element_type.16.up, bf16[1408,256]{1,0:T(8,128)(2,1)} %convert_element_type.17.down, bf16[256,128]{1,0:T(8,128)(2,1)} %convert_element_type.18.pool_in, ...), custom_call_target="tpu_custom_call" | custom-call | tf_op jit(solution)/shard_map/whole_layer/pallas_call | solution.py:886
  236.8 1.8 copy.16
Async XLA Ops:
  0.0 10.7 %copy-start = (f32[256,1408]{1,0:T(8,128)S(1)}, f32[256,1408]{1,0:T(8,128)}, u32[]{:S(2)}) copy-start(f32[256,1408]{1,0:T(8,128)} %param.20) | copy-start | bytes 4325380
  10.7 1.6 copy-start.1

commit v2 on v1

--- a/solution.py
+++ b/solution.py
@@ -449,10 +449,11 @@
 
 
 def layer_kernel(
-    sizes, stream, gate, up, down, pool_in, pool_out, scales, gains, gate_scale, up_scale, down_scale, out,
+    sizes, stream, gate_in, up_in, down_in, in_in, out_in, vectors, out,
+    gate, up, down, pool_in, pool_out, gate_wide, up_wide, down_wide, in_wide, out_wide,
     gate_all, up_all, down_all, in_all, out_all, scales_all, rows_all, first_all, mixed_all, normed,
     gate_sum, up_sum, hidden, pooled, partial, pair, shares,
-    local_sem, z_send, y_send, w_recv, pl_zsend, pl_ysend, pl_recv, slab_send, slab_recv,
+    load_sem, local_sem, z_send, y_send, w_recv, pl_zsend, pl_ysend, pl_recv, slab_send, slab_recv,
     sc_send, sc_recv, ag_send, ag_recv, pair_send, pair_recv, rs_send, rs_recv,
 ):
     rows, small, extra = sizes
@@ -460,7 +461,16 @@
     block = gate.shape[0]
     width = stream.shape[1]
     chans = pool_in.shape[1]
+    units = gate.shape[1]
     features = gate_all.shape[0]
+    starts = [0]
+    for count in (chans, width, width, features, features, features, units, units):
+        starts.append(starts[-1] + count)
+    scales = vectors.at[:, :chans + 2 * width]
+
+    def vector(at, first, count):
+        return vectors[:, pl.ds(pl.multiple_of(starts[at] + first, 128), count)]
+
     every = 2 * rows
     f32, half = jnp.float32, jnp.bfloat16
     fs, tp = lax.axis_index("fs"), lax.axis_index("tp")
@@ -476,11 +486,39 @@
     def upper(at):
         return (((at + 1) // 2) % 2 + core) % 2
 
+    own_rows = pl.ds(pl.multiple_of(low * rows, 16), rows)
+    stream_own = pltpu.make_async_copy(
+        stream, rows_all.at[own_rows, pl.ds(pl.multiple_of(tp * width, 128), width)], local_sem.at[0])
+    stream_own.start()
+    loads = []
+    for i, (wide, ref, narrow) in enumerate((
+        (in_wide, in_in, pool_in), (out_wide, out_in, pool_out), (gate_wide, gate_in, gate),
+        (up_wide, up_in, up), (down_wide, down_in, down),
+    )):
+        copy = pltpu.make_async_copy(ref, wide, load_sem.at[i])
+        copy.start()
+        loads.append((copy, wide, narrow))
+
     barrier = pltpu.get_barrier_semaphore()
     peers = [(2 * at + y, tp) for at in zs[1:]] + [
         (fs_y, tp), (fs, tp_c), (fs, tp_x), (fs, tp_xc), (fs_z, tp_x)]
     for f, t in peers:
         pl.semaphore_signal(barrier, inc=1, device_id={"fs": f, "tp": t}, device_id_type=MESH)
+
+    def narrowed(copy, wide, narrow):
+        copy.wait()
+        count = wide.shape[0]
+        each = 64 if count % 64 == 0 else 16
+
+        def one(i, carry):
+            part = pl.ds(pl.multiple_of(i * each, each), each)
+            narrow[part, :] = wide[part, :].astype(half)
+            return carry
+        lax.fori_loop(0, count // each, one, 0)
+
+    for load in loads:
+        narrowed(*load)
+    stream_own.wait()
     pl.semaphore_wait(barrier, len(peers))
 
     ends = []
@@ -511,37 +549,45 @@
     def subs(at, count):
         return pl.ds(pl.multiple_of(at, 16), count)
 
-    own_rows = subs(low * rows, rows)
-
-    def share_place(ref, chip_low, t, j):
-        return ref.at[subs(chip_low * rows, rows), lanes(t * width + j * block, block)]
-
-    def share_start(phase, ref, j, src):
-        dst = share_place(ref, low, tp, j)
-        chip = 2 * x + low
-        for k, (f, t) in enumerate(((fs_z, tp), (fs, tp_x), (fs_z, tp_x), (fs, tp_c))):
+    pieces = width // block
+
+    def column_block(phase, j, xx, cc):
+        if phase == 0:
+            return (2 * xx + cc) * pieces + j
+        return (2 * j + cc) * pieces + xx
+
+    def share_place(phase, ref, chip_low, j, xx, cc):
+        return ref.at[subs(chip_low * rows, rows), lanes(column_block(phase, j, xx, cc) * block, block)]
+
+    def share_start(phase, ref, j, cond=None):
+        here = share_place(phase, ref, low, j, x, core)
+        for k, (f, t) in enumerate(((fs_z, tp), (fs, tp_x), (fs, tp_c))):
             start(lambda f=f, t=t, k=k: remote(
-                src, dst, ag_send.at[phase, j, k], ag_recv.at[phase, j, chip, core], f, t))
-
-    def share_forward(phase, ref):
-        for j in range(width // block):
-            for k, (cl, t) in enumerate(((1 - low, tp), (low, tp_x), (1 - low, tp_x))):
-                here = share_place(ref, cl, t, j)
-                chip = 2 * (t // 2) + cl
-                arrive(here, ag_recv.at[phase, j, chip, core])
-                start(lambda here=here, chip=chip, k=k, j=j: remote(
-                    here, here, ag_send.at[phase, j, 4 + k], ag_recv.at[phase, j, chip, core], fs, tp_c))
+                here, here, ag_send.at[phase, j, k], ag_recv.at[phase, j, 2 * x + low, core], f, t), cond)
+
+    def share_relay(phase, ref, j, k, chip_low, xx, targets, cond=None):
+        here = share_place(phase, ref, chip_low, j, xx, core)
+        flag = ag_recv.at[phase, j, 2 * xx + chip_low, core]
+        arrive(here, flag, cond)
+        for n, target in enumerate(targets):
+            start(lambda n=n, target=target: remote(
+                here, here, ag_send.at[phase, j, 3 + k + n], flag, fs, target), cond)
+
+    def relay_own(phase, ref, j, cond=None):
+        share_relay(phase, ref, j, 0, 1 - low, x, (tp_x, tp_c), cond)
+
+    def relay_across(phase, ref, j, cond=None):
+        share_relay(phase, ref, j, 2, low, 1 - x, (tp_c,), cond)
+        share_relay(phase, ref, j, 3, 1 - low, 1 - x, (tp_c,), cond)
 
     def share_finish(phase, ref):
-        for j in range(width // block):
-            for cl, t in ((low, tp_c), (1 - low, tp_c), (low, tp_xc), (1 - low, tp_xc)):
-                arrive(share_place(ref, cl, t, j), ag_recv.at[phase, j, 2 * (t // 2) + cl, 1 - core])
-
-    stream_own = pltpu.make_async_copy(
-        stream, rows_all.at[own_rows, lanes(tp * width, width)], local_sem.at[0])
-    stream_own.start()
-    for j in range(width // block):
-        share_start(0, rows_all, j, stream.at[:, j * block:(j + 1) * block])
+        for j in range(2):
+            for xx in (x, 1 - x):
+                for cl in (low, 1 - low):
+                    arrive(share_place(phase, ref, cl, j, xx, 1 - core), ag_recv.at[phase, j, 2 * xx + cl, 1 - core])
+
+    for j in range(2):
+        share_start(0, rows_all, j)
 
     def scale_copy(k, slot, t):
         return remote(scales, scales_all.at[slot], sc_send.at[k], sc_recv.at[slot], fs, t)
@@ -560,13 +606,16 @@
             return in_all.at[:, lanes(t * chans, chans)]
         return out_all.at[subs(t * chans, chans)]
 
+    def pool_start():
+        for which, own in enumerate((pool_in, pool_out)):
+            for k in range(1, 4):
+                start(lambda k=k, which=which, own=own: remote(
+                    own, pool_place(which, fs, tp), pl_zsend.at[which, k], pl_recv.at[which, fs], 2 * zs[k] + y, tp))
+            start(lambda which=which, own=own: remote(
+                own, pool_place(which, fs, tp), pl_ysend.at[which, 0], pl_recv.at[which, fs], fs_y, tp))
+
     for which, own in enumerate((pool_in, pool_out)):
         locals_.append(pltpu.make_async_copy(own, pool_place(which, fs, tp), local_sem.at[2 + which]))
-        for k in range(1, 4):
-            start(lambda k=k, which=which, own=own: remote(
-                own, pool_place(which, fs, tp), pl_zsend.at[which, k], pl_recv.at[which, fs], 2 * zs[4 - k] + y, tp))
-        start(lambda which=which, own=own: remote(
-            own, pool_place(which, fs, tp), pl_ysend.at[which, 0], pl_recv.at[which, fs], fs_y, tp))
 
     def own_part(piece, part, side):
         first, count = (side * small, small) if part == 0 else (2 * small, extra)
@@ -576,7 +625,7 @@
     def all_part(piece, part, f):
         first, count = (0, small) if part == 0 else (small, extra)
         if piece == 2:
-            return down_all.at[f, pl.ds(first, count)]
+            return down_all.at[pl.ds(first, count), lanes(f * block, block)]
         return (gate_all, up_all)[piece].at[subs(f * block, block), pl.ds(first, count)]
 
     def y_own(piece):
@@ -591,15 +640,30 @@
 
     for copy in locals_:
         copy.start()
-    for piece in range(3):
-        for k in (3, 2, 1):
+    inner = (z == 1) | (z == 2)
+
+    def z_own(piece, cond=None, targets=(1, 2, 3)):
+        for k in targets:
             at = zs[k]
             for part in range(2):
-                start(lambda k=k, at=at, part=part, piece=piece: remote(
+                ok = cond
+                if part:
+                    ok = upper(at) == 1 if cond is None else cond & (upper(at) == 1)
+                start(lambda k=k, at=at, part=part: remote(
                     own_part(piece, part, upper(at)), all_part(piece, part, fs), z_send.at[k, piece, part],
-                    w_recv.at[fs, piece, part], 2 * at + y, tp), None if part == 0 else upper(at) == 1)
-        if piece < 2:
-            y_own(piece)
+                    w_recv.at[fs, piece, part], 2 * at + y, tp), ok)
+
+    outer = jnp.logical_not(inner)
+    z_own(0, None, (1,))
+    y_own(0)
+    z_own(1, outer, (1,))
+    z_own(0, None, (2, 3))
+    pool_start()
+    z_own(1, inner, (1,))
+    z_own(1, None, (2, 3))
+    y_own(1)
+    z_own(2, None, (1,))
+    for piece in range(3):
         own_copy(piece, 0).start()
         pl.when(upper(z) == 1)(lambda piece=piece: own_copy(piece, 1).start())
 
@@ -607,7 +671,7 @@
     def _():
         gate_all[:, small:big] = jnp.zeros((features, extra), half)
         up_all[:, small:big] = jnp.zeros((features, extra), half)
-        down_all[:, small:big, :] = jnp.zeros((down_all.shape[0], extra, block), half)
+        down_all[small:big, :] = jnp.zeros((extra, features), half)
 
     def weights_here(piece, f):
         arrive(all_part(piece, 0, f), w_recv.at[f, piece, 0])
@@ -626,186 +690,234 @@
         pl.when(upper(z) == 1)(lambda: own_copy(piece, 1).wait())
 
     step = 32
-
-    def norm_rows(source, gain_row):
+    lane_tiles = features // 128
+
+    def norm_rows(source, gain_at, base=0):
         def one(i, carry):
-            part = pl.ds(pl.multiple_of(i * step, step), step)
-            floats = source[part, :].astype(f32)
-            scale = lax.rsqrt(jnp.mean(floats * floats, axis=-1, keepdims=True) + eps)
-            normed[part, :] = ((floats * scale) * gains[gain_row:gain_row + 1, :]).astype(half)
+            part = pl.ds(pl.multiple_of(base + i * 128, 128), 128)
+            total = jnp.zeros((128, 128), f32)
+            for c in range(lane_tiles):
+                floats = source[part, c * 128:(c + 1) * 128].astype(f32)
+                total = total + floats * floats
+            scale = lax.rsqrt(jnp.sum(total, axis=-1, keepdims=True) * (1.0 / features) + eps)
+            for c in range(lane_tiles):
+                floats = source[part, c * 128:(c + 1) * 128].astype(f32)
+                normed[part, c * 128:(c + 1) * 128] = ((floats * scale) * vector(gain_at, c * 128, 128)).astype(half)
             return carry
         return one
 
-    stream_own.wait()
-    share_forward(0, rows_all)
+    for j in range(2):
+        relay_own(0, rows_all, j)
+    for j in range(2):
+        relay_across(0, rows_all, j)
     share_finish(0, rows_all)
-    lax.fori_loop(0, every // step, norm_rows(rows_all, 0), 0)
-
-    for k in range(1, 4):
+    lax.fori_loop(0, every // 128, norm_rows(rows_all, 3), 0)
+
+    def pool_by_y():
+        for k in range(1, 4):
+            for which in range(2):
+                f = 2 * zs[k] + y
+                here = pool_place(which, f, tp)
+                arrive(here, pl_recv.at[which, f])
+                start(lambda k=k, which=which, here=here, f=f: remote(
+                    here, here, pl_ysend.at[which, k], pl_recv.at[which, f], fs_y, tp))
+
+    tile = 256
+
+    def accumulate(weights, total, f, first):
+        for n in range(big // 128 // 2 + 1):
+            cols = slice(n * tile, min((n + 1) * tile, big))
+            if cols.start < cols.stop:
+                product = jnp.dot(normed[:, lanes(f * block, block)], weights[subs(f * block, block), cols],
+                                  preferred_element_type=f32)
+                total[:, cols] = product if first else total[:, cols] + product
+
+    def pool_across():
         for which in range(2):
-            f = 2 * zs[k] + y
-            here = pool_place(which, f, tp)
-            arrive(here, pl_recv.at[which, f])
-            start(lambda k=k, which=which, here=here, f=f: remote(
-                here, here, pl_ysend.at[which, k], pl_recv.at[which, f], fs_y, tp))
-
-    tile = 256
-
-    def accumulate(weights, total, f, first):
-        def one(i, carry):
-            part = pl.ds(pl.multiple_of(i * tile, tile), tile)
-            product = jnp.dot(normed[part, lanes(f * block, block)], weights[subs(f * block, block), :],
-                              preferred_element_type=f32)
-            total[part, :] = product if first else total[part, :] + product
-            return carry
-        lax.fori_loop(0, every // tile, one, 0)
-
-    for i in range(4):
-        f, g = 2 * zs[i] + y, 2 * zs[i] + 1 - y
-        for piece, (weights, total) in enumerate(((gate_all, gate_sum), (up_all, up_sum))):
+            locals_[1 + which].wait()
+            for k in range(4):
+                f = fs_y if k == 0 else 2 * zs[k] + 1 - y
+                arrive(pool_place(which, f, tp), pl_recv.at[which, f])
+            slab = pool_slab(which, tp)
+            for n, t in enumerate((tp_x, tp_c)):
+                start(lambda which=which, slab=slab, n=n, t=t: remote(
+                    slab, slab, slab_send.at[which, n], slab_recv.at[which, tp], fs, t))
+
+    ahead = [(piece, i) for piece in range(3) for i in range(1, 4)]
+    for piece, (weights, total) in enumerate(((gate_all, gate_sum), (up_all, up_sum))):
+        for i in range(4):
+            f, g = 2 * zs[i] + y, 2 * zs[i] + 1 - y
             if i == 0:
                 own_here(piece)
             accumulate(weights, total, f, i == 0)
-        if i < 3:
-            by_z(0, i + 1)
-            by_z(1, i + 1)
-        else:
-            y_own(2)
-            own_here(2)
-        for piece, (weights, total) in enumerate(((gate_all, gate_sum), (up_all, up_sum))):
+            if 4 * piece + i < 7:
+                by_z(*ahead[4 * piece + i])
             weights_here(piece, g)
             accumulate(weights, total, g, False)
-        if i == 1:
-            for which in range(2):
-                locals_[1 + which].wait()
-                for k in range(4):
-                    if k:
-                        arrive(pool_place(which, 2 * zs[k] + 1 - y, tp), pl_recv.at[which, 2 * zs[k] + 1 - y])
-                    else:
-                        arrive(pool_place(which, fs_y, tp), pl_recv.at[which, fs_y])
-                slab = pool_slab(which, tp)
-                start(lambda which=which, slab=slab: remote(
-                    slab, slab, slab_send.at[which, 0], slab_recv.at[which, tp], fs, tp_x))
-                start(lambda which=which, slab=slab: remote(
-                    slab, slab, slab_send.at[which, 1], slab_recv.at[which, tp], fs, tp_c))
-
-    side = lanes(upper(z) * small, big)
+            if (piece, i) == (0, 2):
+                pool_by_y()
+            if (piece, i) == (0, 3):
+                y_own(2)
+            if (piece, i) == (1, 0):
+                z_own(2, outer, (2, 3))
+                pool_across()
+            if (piece, i) == (1, 1):
+                z_own(2, inner, (2, 3))
+    own_here(2)
 
     def hide(i, carry):
         part = pl.ds(pl.multiple_of(i * step, step), step)
-        a = gate_sum[part, :] * gate_scale[:, side]
-        hidden[part, :] = (a / (1.0 + jnp.exp(-a)) * (up_sum[part, :] * up_scale[:, side])).astype(half)
+        a = gate_sum[part, :] * vector(6, upper(z) * small, big)
+        hidden[part, :] = (a / (1.0 + jnp.exp(-a)) * (up_sum[part, :] * vector(7, upper(z) * small, big))).astype(half)
         return carry
 
     lax.fori_loop(0, every // step, hide, 0)
 
-    def block_product(phase, f):
-        def one(i, carry):
-            part = pl.ds(pl.multiple_of(i * tile, tile), tile)
-            partial[phase, f, part, :] = jnp.dot(
-                hidden[part, :], down_all[f], preferred_element_type=f32).astype(half)
-            return carry
-        lax.fori_loop(0, every // tile, one, 0)
+    sides = ((1 - low) * rows, low * rows)
+
+    def block_send(phase, f, h):
         zz = f // 2
         slot = 2 * (zz // 2) + f % 2
+        part = subs(sides[h], rows)
         start(lambda: remote(
-            partial.at[phase, f], pair.at[phase, slot], pair_send.at[phase, f], pair_recv.at[phase, slot], fs, tp_c),
-            zz % 2 != core)
-
-    def block_sum(phase, f):
+            partial.at[phase, f, part], pair.at[phase, slot, part], pair_send.at[phase, f, h],
+            pair_recv.at[phase, slot, h], fs, tp_c), zz % 2 != core)
+
+    def core_sum(phase, f, h):
         zz = f // 2
         slot = 2 * (zz // 2) + f % 2
-        here, there = subs(low * rows, rows), subs((1 - low) * rows, rows)
 
         @pl.when(zz % 2 == core)
         def _():
-            remote(pair.at[phase, slot], pair.at[phase, slot], pair_send.at[phase, f], pair_recv.at[phase, slot],
-                   fs, tp_c).wait_recv()
+            here = pair.at[phase, slot, subs(sides[h], rows)]
+            remote(here, here, pair_send.at[phase, f, h], pair_recv.at[phase, slot, h], fs, tp_c).wait_recv()
 
             def one(i, carry):
-                part = pl.ds(pl.multiple_of(i * 128, 128), 128)
-                partial[phase, f, part, :] = (
-                    partial[phase, f, part, :].astype(f32) + pair[phase, slot, part, :].astype(f32)).astype(half)
+                at = pl.ds(pl.multiple_of(sides[h] + i * 128, 128), 128)
+                partial[phase, f, at, :] = (
+                    partial[phase, f, at, :].astype(f32) + pair[phase, slot, at, :].astype(f32)).astype(half)
                 return carry
-            lax.fori_loop(0, every // 128, one, 0)
-
-        mine = zz // 2 == x
-        for k, (part, fd, td, cond) in enumerate((
-            (here, fs, tp_x, jnp.logical_not(mine)), (there, fs_z, tp, mine), (there, fs_z, tp_x, jnp.logical_not(mine)),
-        )):
-            start(lambda k=k, part=part, fd=fd, td=td: remote(
-                partial.at[phase, f, part], shares.at[phase, k, f % 2], rs_send.at[phase, slot, k],
-                rs_recv.at[phase, k, f % 2], fd, td), (zz % 2 == core) & cond)
-
-    def block_total(phase, j, resid, target):
-        f = 2 * tp + j
-        for k in range(3):
-            arrive(shares.at[phase, k, j], rs_recv.at[phase, k, j])
-
+            lax.fori_loop(0, rows // 128, one, 0)
+
+    def reduce_send(phase, f, h, k, dst, recv, fd, td, cond):
+        start(lambda: remote(
+            partial.at[phase, f, subs(sides[h], rows)], shares.at[phase, *dst],
+            rs_send.at[phase, 2 * (f // 4) + f % 2, k], rs_recv.at[phase, *recv], fd, td),
+            ((f // 2) % 2 == core) & cond)
+
+    def add_rows(f, phase, dst, target):
         def one(i, carry):
             at = pl.multiple_of(i * 64, 64)
-            total = partial[phase, f, pl.ds(pl.multiple_of(low * rows + at, 64), 64), :].astype(f32)
-            for k in range(3):
-                total = total + shares[phase, k, j, pl.ds(at, 64), :].astype(f32)
-            cols = slice(j * block, (j + 1) * block)
-            target(at, j, (resid(at, j) + total * (0.5 * down_scale[:, cols])).astype(half))
+            here = pl.ds(pl.multiple_of(low * rows + at, 64), 64)
+            total = partial[phase, f, here, :].astype(f32)
+            for place_of in dst:
+                total = total + shares[phase, *place_of, pl.ds(at, 64), :].astype(f32)
+            target(at, here, total)
             return carry
         lax.fori_loop(0, rows // 64, one, 0)
 
-    def stream_part(at, j):
-        return stream[pl.ds(at, 64), j * block:(j + 1) * block].astype(f32)
-
-    def first_part(at, j, value):
-        first_all[pl.ds(pl.multiple_of(low * rows + at, 64), 64), lanes(tp * width + j * block, block)] = value
-
-    def first_done(i):
-        @pl.when(zs[i] == tp)
+    def first_sum(f):
+        for h in range(2):
+            core_sum(0, f, h)
+            if h == 0:
+                to = (f // 4, f % 2)
+                reduce_send(0, f, 0, 0, to, to, fs_z, tp, True)
+
+    def first_middle(f):
+        q, j = f // 4, f % 2
+
+        @pl.when((f // 2) % 2 == core)
         def _():
-            for j in range(2):
-                block_total(0, j, stream_part, first_part)
-
-    by_z(2, 1)
-    for i in range(4):
-        f, g = 2 * zs[i] + y, 2 * zs[i] + 1 - y
-        block_product(0, f)
-        block_sum(0, f)
-        if 1 <= i < 3:
-            by_z(2, i + 1)
-        if i == 1:
-            for which in range(2):
-                slab = pool_slab(which, tp_x)
-                arrive(slab, slab_recv.at[which, tp_x])
-                start(lambda which=which, slab=slab: remote(
-                    slab, slab, slab_send.at[which, 2], slab_recv.at[which, tp_x], fs, tp_c))
-        weights_here(2, g)
-        block_product(0, g)
-        block_sum(0, g)
-        if i == 2:
-            first_done(0)
-            first_done(1)
-        if i == 3:
-            first_done(2)
-            first_done(3)
-    for j in range(2):
-        share_start(1, first_all, j, share_place(first_all, low, tp, j))
+            here = shares.at[0, q, j]
+            remote(here, here, rs_recv.at[0, q, j], rs_recv.at[0, q, j], fs, tp_c).wait_recv()
+
+            def target(at, here, total):
+                partial[0, f, here, :] = total.astype(half)
+            add_rows(f, 0, ((q, j),), target)
+        reduce_send(0, f, 1, 1, (2, q), (2, q), fs, tp_x, j != x)
+
+    def first_done(f):
+        q, j = f // 4, f % 2
+        cond = ((f // 2) % 2 == core) & (j == x)
+
+        @pl.when(cond)
+        def _():
+            here = shares.at[0, 2, q]
+            remote(here, here, rs_recv.at[0, 2, q], rs_recv.at[0, 2, q], fs, tp_c).wait_recv()
+            cols = lanes(f * block, block)
+            factor = 0.5 * scales_all[f // 2, :, pl.ds(pl.multiple_of(chans + width + j * block, 128), block)]
+
+            def target(at, here, total):
+                first_all[here, cols] = (rows_all[here, cols].astype(f32) + total * factor).astype(half)
+            add_rows(f, 0, ((2, q),), target)
+        share_start(1, first_all, q, cond)
+
+    def first_relay(f):
+        q, j = f // 4, f % 2
+        turn = (f // 2) % 2 == core
+        relay_own(1, first_all, q, turn & (j == x))
+        relay_across(1, first_all, q, turn & (j != x))
+
+    def second_sum(f, h):
+        core_sum(1, f, h)
+        mine = f // 4 == x
+        away = jnp.logical_not(mine)
+        if h == 0:
+            reduce_send(1, f, 0, 1, (1, f % 2), (1, f % 2), fs_z, tp, mine)
+            reduce_send(1, f, 0, 2, (2, f % 2), (2, f % 2), fs_z, tp_x, away)
+        else:
+            reduce_send(1, f, 1, 0, (0, f % 2), (0, f % 2), fs, tp_x, away)
+
+    blocks = [2 * zs[i] + j for i in range(4) for j in (y, 1 - y)]
+
+    def slab_across():
+        for which in range(2):
+            slab = pool_slab(which, tp_x)
+            arrive(slab, slab_recv.at[which, tp_x])
+            start(lambda which=which, slab=slab: remote(
+                slab, slab, slab_send.at[which, 2], slab_recv.at[which, tp_x], fs, tp_c))
+
+    locals_[0].wait()
+    for t in (tp_c, tp_x, tp_xc):
+        arrive(scales_all.at[t], sc_recv.at[t])
+    for n, f in enumerate(blocks):
+        if n % 2:
+            weights_here(2, f)
+        partial[0, f, :, :] = jnp.dot(
+            hidden[...], down_all[:, lanes(f * block, block)], preferred_element_type=f32).astype(half)
+        for h in range(2):
+            block_send(0, f, h)
+        if n in (0, 2):
+            by_z(2, 2 + n // 2)
+        first_sum(f)
+        if n == 3:
+            slab_across()
+        for m in {4: (0, 2), 5: (1, 3), 6: (4,), 7: (5,)}.get(n, ()):
+            first_middle(blocks[m])
+        for m in {6: (0, 2), 7: (1, 3)}.get(n, ()):
+            first_done(blocks[m])
+    first_middle(blocks[6])
+    first_done(blocks[4])
+    first_middle(blocks[7])
+    for m in (0, 2, 1, 3):
+        first_relay(blocks[m])
+    for m in (5, 6, 7):
+        first_done(blocks[m])
+        first_relay(blocks[m - 1])
+    first_relay(blocks[7])
     for which in range(2):
         for t in (tp_c, tp_xc):
             arrive(pool_slab(which, t), slab_recv.at[which, t])
-    locals_[0].wait()
-    for t in (tp_c, tp_x, tp_xc):
-        arrive(scales_all.at[t], sc_recv.at[t])
-    share_forward(1, first_all)
     share_finish(1, first_all)
 
     in_scale = jnp.concatenate([scales_all[t, :, :chans] for t in range(4)], axis=1)
-    lax.fori_loop(0, every // step, norm_rows(first_all, 1), 0)
     group = 4 * chans // 4
     pos_row = lax.broadcasted_iota(jnp.int32, (SEQ, SEQ), 0)
     pos_col = lax.broadcasted_iota(jnp.int32, (SEQ, SEQ), 1)
     pos = lax.broadcasted_iota(jnp.int32, (SEQ, 1), 0)
 
-    def mix(h, carry):
-        base = pl.multiple_of(h * rows, rows)
+    def mix(h):
+        base = pl.multiple_of(sides[h], 128)
         part = pl.ds(base, rows)
         pool_input = (jnp.dot(normed[part, :], in_all[...], preferred_element_type=f32) * in_scale).astype(half)
         for index, window in enumerate(WINDOWS):
@@ -823,35 +935,36 @@
             cols = slice(t * width, (t + 1) * width)
             mixed = jnp.dot(pooled[...], out_all[:, cols], preferred_element_type=f32)
             mixed_all[part, cols] = (
-                first_all[part, cols].astype(f32) + mixed * scales_all[t, :, chans:]).astype(half)
-        return carry
-
-    lax.fori_loop(0, 2, mix, 0)
-    lax.fori_loop(0, every // step, norm_rows(mixed_all, 2), 0)
-
-    def both(i, carry):
-        part = pl.ds(pl.multiple_of(i * tile, tile), tile)
-        a = jnp.dot(normed[part, :], gate_all[...], preferred_element_type=f32) * gate_scale[:, side]
-        b = jnp.dot(normed[part, :], up_all[...], preferred_element_type=f32) * up_scale[:, side]
+                first_all[part, cols].astype(f32) + mixed * scales_all[t, :, chans:chans + width]).astype(half)
+
+    order = [2 * xx + cc for cc in (1 - core, core) for xx in (1 - x, x)]
+    for h in range(2):
+        lax.fori_loop(0, rows // 128, norm_rows(first_all, 4, sides[h]), 0)
+        mix(h)
+        lax.fori_loop(0, rows // 128, norm_rows(mixed_all, 5, sides[h]), 0)
+        part = subs(sides[h], rows)
+        a = jnp.dot(normed[part, :], gate_all[...], preferred_element_type=f32) * vector(6, upper(z) * small, big)
+        b = jnp.dot(normed[part, :], up_all[...], preferred_element_type=f32) * vector(7, upper(z) * small, big)
         hidden[part, :] = (a / (1.0 + jnp.exp(-a)) * b).astype(half)
-        return carry
-
-    lax.fori_loop(0, every // tile, both, 0)
-    order = [2 * zz + j for zz in (2 * (1 - x), 2 * (1 - x) + 1, 2 * x, 2 * x + 1) for j in range(2)]
-    for k, f in enumerate(order):
-        block_product(1, f)
-        if k:
-            block_sum(1, order[k - 1])
-    block_sum(1, order[-1])
-
-    def mixed_part(at, j):
-        return mixed_all[pl.ds(pl.multiple_of(low * rows + at, 64), 64), lanes(tp * width + j * block, block)].astype(f32)
-
-    def out_part(at, j, value):
-        out[pl.ds(at, 64), j * block:(j + 1) * block] = value
+        for n, zz in enumerate(order):
+            product = jnp.dot(hidden[part, :], down_all[:, lanes(zz * width, width)], preferred_element_type=f32)
+            for j in range(2):
+                partial[1, 2 * zz + j, part, :] = product[:, j * block:(j + 1) * block].astype(half)
+            for j in range(2):
+                block_send(1, 2 * zz + j, h)
+            if n > 1:
+                for j in range(2):
+                    second_sum(2 * zz + j, h)
 
     for j in range(2):
-        block_total(1, j, mixed_part, out_part)
+        for k in range(3):
+            arrive(shares.at[1, k, j], rs_recv.at[1, k, j])
+
+        def target(at, here, total, j=j):
+            value = mixed_all[here, lanes(tp * width + j * block, block)].astype(f32)
+            factor = 0.5 * vector(2, j * block, block)
+            out[pl.ds(at, 64), j * block:(j + 1) * block] = (value + total * factor).astype(half)
+        add_rows(2 * tp + j, 1, ((0, j), (1, j), (2, j)), target)
 
     for make, cond in ends:
         if cond is None:
@@ -871,7 +984,7 @@
     )
 
 
-def whole_layer(stream, gains, gate, gate_scale, up, up_scale, down, down_scale, pool_in, pool_out, scales):
+def whole_layer(stream, gate, up, down, pool_in, pool_out, vectors):
     rows, width = stream.shape
     block, units = gate.shape
     chans = pool_in.shape[1]
@@ -882,32 +995,33 @@
     every = 2 * rows
     f32, half = jnp.float32, jnp.bfloat16
     vmem = pl.BlockSpec(memory_space=pltpu.VMEM)
+    hbm = pl.BlockSpec(memory_space=pl.ANY)
     dma = pltpu.SemaphoreType.DMA
+    weights = (gate, up, down, pool_in, pool_out)
     return pl.pallas_call(
         functools.partial(layer_kernel, (rows, small, extra)),
         name="whole_layer",
         out_shape=jax.ShapeDtypeStruct((rows, width), half),
-        in_specs=[vmem] * 11,
+        in_specs=[hbm] * 6 + [vmem],
         out_specs=vmem,
-        scratch_shapes=[
-            pltpu.VMEM((features, big), half), pltpu.VMEM((features, big), half), pltpu.VMEM((8, big, block), half),
+        scratch_shapes=[pltpu.VMEM(w.shape, half) for w in weights] + [pltpu.VMEM(w.shape, f32) for w in weights] + [
+            pltpu.VMEM((features, big), half), pltpu.VMEM((features, big), half), pltpu.VMEM((big, features), half),
             pltpu.VMEM((features, 4 * chans), half), pltpu.VMEM((4 * chans, features), half),
-            pltpu.VMEM((4,) + scales.shape, f32),
+            pltpu.VMEM((4, 1, chans + 2 * width), f32),
             pltpu.VMEM((every, features), half), pltpu.VMEM((every, features), half),
             pltpu.VMEM((every, features), half), pltpu.VMEM((every, features), half),
             pltpu.VMEM((every, big), f32), pltpu.VMEM((every, big), f32), pltpu.VMEM((every, big), half),
             pltpu.VMEM((rows, 4 * chans), half),
             pltpu.VMEM((2, 8, every, block), half), pltpu.VMEM((2, 4, every, block), half),
             pltpu.VMEM((2, 3, 2, rows, block), half),
-            dma((10,)), dma((4, 3, 2)), dma((4, 3, 2)), dma((8, 3, 2)),
+            dma((5,)), dma((10,)), dma((4, 3, 2)), dma((4, 3, 2)), dma((8, 3, 2)),
             dma((2, 4)), dma((2, 4)), dma((2, 8)), dma((2, 3)), dma((2, 4)),
             dma((3,)), dma((4,)), dma((2, 2, 7)), dma((2, 2, 4, 2)),
-            dma((2, 8)), dma((2, 4)), dma((2, 4, 3)), dma((2, 3, 2)),
+            dma((2, 8, 2)), dma((2, 4, 2)), dma((2, 4, 3)), dma((2, 3, 2)),
         ],
         compiler_params=pltpu.CompilerParams(
-            collective_id=0, has_side_effects=True, vmem_limit_bytes=58 << 20),
-    )(stream, gate, up, down, pool_in, pool_out, scales, gains, gate_scale.reshape(1, -1), up_scale.reshape(1, -1),
-      down_scale.reshape(1, -1))
+            collective_id=0, has_side_effects=True, vmem_limit_bytes=60 << 20),
+    )(stream, *weights, vectors)
 
 
 def body(
@@ -917,13 +1031,14 @@
     pool_in_weight, pool_in_scale, pool_out_weight, pool_out_scale,
 ):
     half = jnp.bfloat16
+    if fits(nfs, ntp, stream, gate_weight, pool_in_weight):
+        vectors = jnp.concatenate([
+            pool_in_scale, pool_out_scale, down_scale, gain_first, gain_mixer, gain_second, gate_scale, up_scale])
+        return whole_layer(
+            stream, gate_weight, up_weight, down_weight, pool_in_weight, pool_out_weight, vectors.reshape(1, -1))
     in_half, out_half = pool_in_weight.astype(half), pool_out_weight.astype(half)
     width, channels = stream.shape[1], in_half.shape[1]
     scales = jnp.concatenate([pool_in_scale, pool_out_scale]).reshape(1, -1)
-    if fits(nfs, ntp, stream, gate_weight, pool_in_weight):
-        return whole_layer(
-            stream, jnp.stack([gain_first, gain_mixer, gain_second]), gate_weight.astype(half), gate_scale,
-            up_weight.astype(half), up_scale, down_weight.astype(half), down_scale, in_half, out_half, scales)
     in_all, out_all, gate_all, up_all, down_all, stream_all, scales_all = gather_all(
         nfs, ntp, in_half, out_half, gate_weight.astype(half), up_weight.astype(half), down_weight.astype(half),
         stream, scales,

time: 241 us -> 204 us (0.85)
  Pallas kernels: 224 us -> 192 us
  other arithmetic: 9.42 us -> 0.01 us
    pallas_call x1, Pallas kernels: 224 us -> 192 us  [whole_layer(): pl.pallas_call(functools.partial(layer_kernel, (rows, small, extra)), nam...]
    convert_element_type x5 -> x0, other arithmetic: 7.26 us -> none  [the longest x1 2.3 us: body(): gate_weight.astype(half)]
    unnamed x5 -> x8, local copies, waits for them, and re-layouts: 2.45 us -> 6.61 us
    reshape x3 -> x1, local copies, waits for them, and re-layouts: 3.19 us -> 0.64 us  [body(): vectors.reshape(1, -1)]
where the time goes in v2:
time: 204 us; the launch traced here: 200 us
  Pallas kernels  192 us (94%)
  local copies, waits for them, and re-layouts  7.96 us (4%)
    pallas_call x1, Pallas kernels, whole_layer(): pl.pallas_call(functools.partial(layer_kernel, (rows, small, extra)), nam...  192 us
    unnamed x8, local copies, waits for them, and re-layouts  6.61 us

profile of v2, /device:TPU:0, one launch (start us, length us, event | category | flops | bytes accessed | tf_op | source)
XLA Modules:
  0.0 200.3 jit_solution(562553308096888690)
XLA Ops:
  0.0 0.7 constant_dynamic-update-slice_fusion.7
  0.7 0.7 constant_dynamic-update-slice_fusion.6
  1.3 0.7 constant_dynamic-update-slice_fusion.5
  2.0 0.7 constant_dynamic-update-slice_fusion.4
  2.7 0.7 constant_dynamic-update-slice_fusion.3
  3.4 0.7 constant_dynamic-update-slice_fusion.2
  4.1 0.7 constant_dynamic-update-slice_fusion.1
  4.9 0.7 constant_dynamic-update-slice_fusion
  5.6 0.6 reshape.3.vectors
  6.2 192.3 %whole_layer.1 = bf16[384,512]{1,0:T(8,128)(2,1)} custom-call(bf16[384,512]{1,0:T(8,128)(2,1)} %stream.1, f32[256,1408]{1,0:T(8,128)} %gate_in.1, f32[256,1408]{1,0:T(8,128)} %up_in.1, f32[1408,256]{1,0:T(8,128)} %down_in.1, f32[256,128]{1,0:T(8,128)} %in_in.1, f32[128,256]{1,0:T(8,128)} %out_in.1, f32[1,10112]{1,0:T(1,128)} %reshape.3.vectors), custom_call_target="tpu_custom_call" | custom-call | tf_op jit(solution)/shard_map/whole_layer/pallas_call | solution.py:1001
  198.6 1.8 copy.24
  (1 shorter events, 0.0 us)

commit v3 on v2

--- a/solution.py
+++ b/solution.py
@@ -12,6 +12,7 @@
 
 eps = 1e-06
 WINDOWS = (2, 4, 8, 16)
+Z_FIRST = (5, 7)
 
 
 def fs_grid(count):
@@ -449,12 +450,19 @@
 
 
 def layer_kernel(
-    sizes, stream, gate_in, up_in, down_in, in_in, out_in, vectors, out,
+    sizes, stream, gate_in, up_in, down_in, in_in, out_in, *refs):
+    parts, (out, vectors, *rest) = refs[:8], refs[8:]
+    layer_steps(sizes, stream, gate_in, up_in, down_in, in_in, out_in, parts, out, vectors, *rest)
+
+
+def layer_steps(
+    sizes, stream, gate_in, up_in, down_in, in_in, out_in, parts, out, vectors,
     gate, up, down, pool_in, pool_out, gate_wide, up_wide, down_wide, in_wide, out_wide,
     gate_all, up_all, down_all, in_all, out_all, scales_all, rows_all, first_all, mixed_all, normed,
-    gate_sum, up_sum, hidden, pooled, partial, pair, shares,
-    load_sem, local_sem, z_send, y_send, w_recv, pl_zsend, pl_ysend, pl_recv, slab_send, slab_recv,
-    sc_send, sc_recv, ag_send, ag_recv, pair_send, pair_recv, rs_send, rs_recv,
+    gate_sum, up_sum, hidden, pooled, partial, pair, shares, first_in,
+    load_sem, vector_sem, local_sem, z_send, y_send, w_recv, pl_zsend, pl_ysend, pl_recv, slab_send, slab_recv,
+    sc_send, sc_recv, ag_send, ag_recv, pair_send, pair_recv, two_send, two_recv, rs_send, rs_recv,
+    fr_send, fr_recv, fr_core,
 ):
     rows, small, extra = sizes
     big = small + extra
@@ -490,6 +498,11 @@
     stream_own = pltpu.make_async_copy(
         stream, rows_all.at[own_rows, pl.ds(pl.multiple_of(tp * width, 128), width)], local_sem.at[0])
     stream_own.start()
+    vector_copies = [
+        pltpu.make_async_copy(ref, vectors.at[0, pl.ds(first, ref.shape[0])], vector_sem.at[i])
+        for i, (ref, first) in enumerate(zip(parts, starts))]
+    for copy in vector_copies:
+        copy.start()
     loads = []
     for i, (wide, ref, narrow) in enumerate((
         (in_wide, in_in, pool_in), (out_wide, out_in, pool_out), (gate_wide, gate_in, gate),
@@ -519,6 +532,8 @@
     for load in loads:
         narrowed(*load)
     stream_own.wait()
+    for copy in vector_copies:
+        copy.wait()
     pl.semaphore_wait(barrier, len(peers))
 
     ends = []
@@ -534,6 +549,14 @@
         else:
             pl.when(cond)(lambda: make().start())
         ends.append((make, cond))
+
+    def flush():
+        for make, cond in ends:
+            if cond is None:
+                make().wait_send()
+            else:
+                pl.when(cond)(lambda make=make: make().wait_send())
+        ends.clear()
 
     def arrive(dst, recv, cond=None):
         def wait():
@@ -551,13 +574,11 @@
 
     pieces = width // block
 
-    def column_block(phase, j, xx, cc):
-        if phase == 0:
-            return (2 * xx + cc) * pieces + j
-        return (2 * j + cc) * pieces + xx
+    def column_block(j, xx, cc):
+        return (2 * xx + cc) * pieces + j
 
     def share_place(phase, ref, chip_low, j, xx, cc):
-        return ref.at[subs(chip_low * rows, rows), lanes(column_block(phase, j, xx, cc) * block, block)]
+        return ref.at[subs(chip_low * rows, rows), lanes(column_block(j, xx, cc) * block, block)]
 
     def share_start(phase, ref, j, cond=None):
         here = share_place(phase, ref, low, j, x, core)
@@ -773,102 +794,131 @@
 
     lax.fori_loop(0, every // step, hide, 0)
 
-    sides = ((1 - low) * rows, low * rows)
-
-    def block_send(phase, f, h):
+    def block_send(f, r):
         zz = f // 2
         slot = 2 * (zz // 2) + f % 2
-        part = subs(sides[h], rows)
+        part = subs(r * rows, rows)
         start(lambda: remote(
-            partial.at[phase, f, part], pair.at[phase, slot, part], pair_send.at[phase, f, h],
-            pair_recv.at[phase, slot, h], fs, tp_c), zz % 2 != core)
-
-    def core_sum(phase, f, h):
-        zz = f // 2
-        slot = 2 * (zz // 2) + f % 2
-
-        @pl.when(zz % 2 == core)
+            partial.at[f, part], pair.at[0, slot, part], pair_send.at[f, r],
+            pair_recv.at[slot, r], fs, tp_c), zz % 2 != core)
+
+    def core_sum(f, r):
+        slot = 2 * (f // 4) + f % 2
+
+        @pl.when((f // 2) % 2 == core)
         def _():
-            here = pair.at[phase, slot, subs(sides[h], rows)]
-            remote(here, here, pair_send.at[phase, f, h], pair_recv.at[phase, slot, h], fs, tp_c).wait_recv()
+            here = pair.at[0, slot, subs(r * rows, rows)]
+            remote(here, here, pair_send.at[f, r], pair_recv.at[slot, r], fs, tp_c).wait_recv()
 
             def one(i, carry):
-                at = pl.ds(pl.multiple_of(sides[h] + i * 128, 128), 128)
-                partial[phase, f, at, :] = (
-                    partial[phase, f, at, :].astype(f32) + pair[phase, slot, at, :].astype(f32)).astype(half)
+                at = pl.ds(pl.multiple_of(r * rows + i * 128, 128), 128)
+                partial[f, at, :] = (
+                    partial[f, at, :].astype(f32) + pair[0, slot, at, :].astype(f32)).astype(half)
                 return carry
             lax.fori_loop(0, rows // 128, one, 0)
 
-    def reduce_send(phase, f, h, k, dst, recv, fd, td, cond):
-        start(lambda: remote(
-            partial.at[phase, f, subs(sides[h], rows)], shares.at[phase, *dst],
-            rs_send.at[phase, 2 * (f // 4) + f % 2, k], rs_recv.at[phase, *recv], fd, td),
-            ((f // 2) % 2 == core) & cond)
-
-    def add_rows(f, phase, dst, target):
-        def one(i, carry):
-            at = pl.multiple_of(i * 64, 64)
-            here = pl.ds(pl.multiple_of(low * rows + at, 64), 64)
-            total = partial[phase, f, here, :].astype(f32)
-            for place_of in dst:
-                total = total + shares[phase, *place_of, pl.ds(at, 64), :].astype(f32)
-            target(at, here, total)
-            return carry
-        lax.fori_loop(0, rows // 64, one, 0)
-
-    def first_sum(f):
-        for h in range(2):
-            core_sum(0, f, h)
-            if h == 0:
-                to = (f // 4, f % 2)
-                reduce_send(0, f, 0, 0, to, to, fs_z, tp, True)
-
-    def first_middle(f):
-        q, j = f // 4, f % 2
+    blocks = [2 * zs[i] + j for i in range(4) for j in (y, 1 - y)]
+
+    def ways(n):
+        across_x, across_z = (fs, tp_x), (fs_z, tp)
+        return (across_z, across_x, low) if n in Z_FIRST else (across_x, across_z, x)
+
+    def first_send(n, k, src, dst, recv, to):
+        f = blocks[n]
+        start(lambda: remote(src, dst, fr_send.at[2 * (f // 4) + f % 2, k], recv, *to), (f // 2) % 2 == core)
+
+    def first_sum(n):
+        f = blocks[n]
+        slot = 2 * (f // 4) + f % 2
+        to, _, r = ways(n)
+        core_sum(f, 1 - r)
+        first_send(n, 0, partial.at[f, subs((1 - r) * rows, rows)], first_in.at[0, slot], fr_recv.at[slot, 0], to)
+        core_sum(f, r)
+
+    def first_add(n):
+        f = blocks[n]
+        slot = 2 * (f // 4) + f % 2
+        _, to, r = ways(n)
+        part = subs(r * rows, rows)
 
         @pl.when((f // 2) % 2 == core)
         def _():
-            here = shares.at[0, q, j]
-            remote(here, here, rs_recv.at[0, q, j], rs_recv.at[0, q, j], fs, tp_c).wait_recv()
-
-            def target(at, here, total):
-                partial[0, f, here, :] = total.astype(half)
-            add_rows(f, 0, ((q, j),), target)
-        reduce_send(0, f, 1, 1, (2, q), (2, q), fs, tp_x, j != x)
-
-    def first_done(f):
-        q, j = f // 4, f % 2
-        cond = ((f // 2) % 2 == core) & (j == x)
-
-        @pl.when(cond)
+            arrive(first_in.at[0, slot], fr_recv.at[slot, 0])
+
+            def one(i, carry):
+                at = pl.ds(pl.multiple_of(r * rows + i * 128, 128), 128)
+                got = first_in[0, slot, pl.ds(pl.multiple_of(i * 128, 128), 128), :].astype(f32)
+                partial[f, at, :] = (partial[f, at, :].astype(f32) + got).astype(half)
+                return carry
+            lax.fori_loop(0, rows // 128, one, 0)
+        first_send(n, 1, partial.at[f, part], first_in.at[1, slot], fr_recv.at[slot, 1], to)
+
+    def first_done(n):
+        f = blocks[n]
+        slot = 2 * (f // 4) + f % 2
+        to, _, r = ways(n)
+        cols = lanes(f * block, block)
+
+        @pl.when((f // 2) % 2 == core)
         def _():
-            here = shares.at[0, 2, q]
-            remote(here, here, rs_recv.at[0, 2, q], rs_recv.at[0, 2, q], fs, tp_c).wait_recv()
-            cols = lanes(f * block, block)
-            factor = 0.5 * scales_all[f // 2, :, pl.ds(pl.multiple_of(chans + width + j * block, 128), block)]
-
-            def target(at, here, total):
-                first_all[here, cols] = (rows_all[here, cols].astype(f32) + total * factor).astype(half)
-            add_rows(f, 0, ((2, q),), target)
-        share_start(1, first_all, q, cond)
-
-    def first_relay(f):
-        q, j = f // 4, f % 2
-        turn = (f // 2) % 2 == core
-        relay_own(1, first_all, q, turn & (j == x))
-        relay_across(1, first_all, q, turn & (j != x))
-
-    def second_sum(f, h):
-        core_sum(1, f, h)
+            arrive(first_in.at[1, slot], fr_recv.at[slot, 1])
+            factor = 0.5 * scales_all[f // 2, :, pl.ds(pl.multiple_of(chans + width + (f % 2) * block, 128), block)]
+
+            def one(i, carry):
+                at = pl.ds(pl.multiple_of(r * rows + i * 128, 128), 128)
+                total = partial[f, at, :].astype(f32) + first_in[
+                    1, slot, pl.ds(pl.multiple_of(i * 128, 128), 128), :].astype(f32)
+                first_all[at, cols] = (rows_all[at, cols].astype(f32) + total * factor).astype(half)
+                return carry
+            lax.fori_loop(0, rows // 128, one, 0)
+        here = first_all.at[subs(r * rows, rows), cols]
+        first_send(n, 2, here, here, fr_recv.at[slot, 2], to)
+        first_send(n, 3, here, here, fr_core.at[slot, r], (fs, tp_c))
+
+    def first_pass(n):
+        f = blocks[n]
+        slot = 2 * (f // 4) + f % 2
+        r = 1 - ways(n)[2]
+        here = first_all.at[subs(r * rows, rows), lanes(f * block, block)]
+        arrive(here, fr_recv.at[slot, 2], (f // 2) % 2 == core)
+        first_send(n, 4, here, here, fr_core.at[slot, r], (fs, tp_c))
+
+    def first_finish():
+        for f in blocks:
+            slot = 2 * (f // 4) + f % 2
+            for r in range(2):
+                arrive(first_all.at[r * rows:(r + 1) * rows, lanes(f * block, block)], fr_core.at[slot, r],
+                       (f // 2) % 2 != core)
+
+    def part_send(f, h, c, base, count):
+        slot = 2 * (f // 4) + f % 2
+        part = subs(base, count)
+        start(lambda: remote(
+            partial.at[f, part], pair.at[1, slot, part], two_send.at[f, h, c], two_recv.at[slot, h, c], fs, tp_c),
+            (f // 2) % 2 != core)
+
+    def part_sum(f, h, c, base, first, count):
+        slot = 2 * (f // 4) + f % 2
+        part = subs(base, count)
+
+        @pl.when((f // 2) % 2 == core)
+        def _():
+            arrive(pair.at[1, slot, part], two_recv.at[slot, h, c])
+
+            def one(i, carry):
+                at = pl.ds(pl.multiple_of(base + i * 128, 128), 128)
+                partial[f, at, :] = (partial[f, at, :].astype(f32) + pair[1, slot, at, :].astype(f32)).astype(half)
+                return carry
+            lax.fori_loop(0, count // 128, one, 0)
         mine = f // 4 == x
         away = jnp.logical_not(mine)
-        if h == 0:
-            reduce_send(1, f, 0, 1, (1, f % 2), (1, f % 2), fs_z, tp, mine)
-            reduce_send(1, f, 0, 2, (2, f % 2), (2, f % 2), fs_z, tp_x, away)
-        else:
-            reduce_send(1, f, 1, 0, (0, f % 2), (0, f % 2), fs, tp_x, away)
-
-    blocks = [2 * zs[i] + j for i in range(4) for j in (y, 1 - y)]
+        ways = ((1, fs_z, tp, mine), (2, fs_z, tp_x, away)) if h == 0 else ((0, fs, tp_x, away),)
+        for k, fd, td, cond in ways:
+            start(lambda k=k, fd=fd, td=td: remote(
+                partial.at[f, part], shares.at[k, f % 2, pl.ds(first, count)], rs_send.at[slot, k, c],
+                rs_recv.at[k, f % 2, c], fd, td), ((f // 2) % 2 == core) & cond)
+
+    cuts = (((0, SEQ), (SEQ, rows - SEQ)), ((0, rows - SEQ), (rows - SEQ, SEQ)))
 
     def slab_across():
         for which in range(2):
@@ -883,32 +933,32 @@
     for n, f in enumerate(blocks):
         if n % 2:
             weights_here(2, f)
-        partial[0, f, :, :] = jnp.dot(
+        partial[f, :, :] = jnp.dot(
             hidden[...], down_all[:, lanes(f * block, block)], preferred_element_type=f32).astype(half)
-        for h in range(2):
-            block_send(0, f, h)
-        if n in (0, 2):
-            by_z(2, 2 + n // 2)
-        first_sum(f)
-        if n == 3:
+        for r in (1 - ways(n)[2], ways(n)[2]):
+            block_send(f, r)
+        first_sum(n)
+        if n == 2:
             slab_across()
-        for m in {4: (0, 2), 5: (1, 3), 6: (4,), 7: (5,)}.get(n, ()):
-            first_middle(blocks[m])
-        for m in {6: (0, 2), 7: (1, 3)}.get(n, ()):
-            first_done(blocks[m])
-    first_middle(blocks[6])
-    first_done(blocks[4])
-    first_middle(blocks[7])
-    for m in (0, 2, 1, 3):
-        first_relay(blocks[m])
-    for m in (5, 6, 7):
-        first_done(blocks[m])
-        first_relay(blocks[m - 1])
-    first_relay(blocks[7])
+        if n in (3, 4):
+            by_z(2, n - 1)
+        for stage, members in {
+            1: ((first_add, (0,)),), 2: ((first_add, (1,)),), 3: ((first_add, (2, 3)),),
+            4: ((first_done, (0, 2, 1, 3)),), 5: ((first_add, (4,)), (first_pass, (0, 2))),
+            6: ((first_add, (5,)), (first_pass, (1, 3))), 7: ((first_done, (4,)), (first_add, (6, 7))),
+        }.get(n, ()):
+            for m in members:
+                stage(m)
+    for stage, m in (
+        (first_done, 5), (first_pass, 4), (first_done, 6), (first_pass, 5), (first_done, 7), (first_pass, 6),
+        (first_pass, 7),
+    ):
+        stage(m)
     for which in range(2):
         for t in (tp_c, tp_xc):
             arrive(pool_slab(which, t), slab_recv.at[which, t])
-    share_finish(1, first_all)
+    first_finish()
+    flush()
 
     in_scale = jnp.concatenate([scales_all[t, :, :chans] for t in range(4)], axis=1)
     group = 4 * chans // 4
@@ -916,9 +966,8 @@
     pos_col = lax.broadcasted_iota(jnp.int32, (SEQ, SEQ), 1)
     pos = lax.broadcasted_iota(jnp.int32, (SEQ, 1), 0)
 
-    def mix(h):
-        base = pl.multiple_of(sides[h], 128)
-        part = pl.ds(base, rows)
+    def mix(base, count):
+        part = pl.ds(pl.multiple_of(base, 128), count)
         pool_input = (jnp.dot(normed[part, :], in_all[...], preferred_element_type=f32) * in_scale).astype(half)
         for index, window in enumerate(WINDOWS):
             before = window // 2
@@ -926,51 +975,58 @@
             last = jnp.minimum(pos_row + window - before, SEQ)
             members = jnp.where((pos_col >= first) & (pos_col < last), 1.0, 0.0).astype(half)
             counts = (jnp.minimum(pos + window - before, SEQ) - jnp.maximum(pos - before, 0)).astype(f32)
-            for s in range(rows // SEQ):
+            for s in range(count // SEQ):
                 own = pool_input[s * SEQ:(s + 1) * SEQ, index * group:(index + 1) * group]
                 sums = jnp.dot(members, own, preferred_element_type=f32)
                 pooled[s * SEQ:(s + 1) * SEQ, index * group:(index + 1) * group] = (
                     sums / counts - own.astype(f32)).astype(half)
         for t in range(4):
             cols = slice(t * width, (t + 1) * width)
-            mixed = jnp.dot(pooled[...], out_all[:, cols], preferred_element_type=f32)
+            mixed = jnp.dot(pooled[:count, :], out_all[:, cols], preferred_element_type=f32)
             mixed_all[part, cols] = (
                 first_all[part, cols].astype(f32) + mixed * scales_all[t, :, chans:chans + width]).astype(half)
 
     order = [2 * xx + cc for cc in (1 - core, core) for xx in (1 - x, x)]
+    sides = (1 - low, low)
     for h in range(2):
-        lax.fori_loop(0, rows // 128, norm_rows(first_all, 4, sides[h]), 0)
-        mix(h)
-        lax.fori_loop(0, rows // 128, norm_rows(mixed_all, 5, sides[h]), 0)
-        part = subs(sides[h], rows)
-        a = jnp.dot(normed[part, :], gate_all[...], preferred_element_type=f32) * vector(6, upper(z) * small, big)
-        b = jnp.dot(normed[part, :], up_all[...], preferred_element_type=f32) * vector(7, upper(z) * small, big)
-        hidden[part, :] = (a / (1.0 + jnp.exp(-a)) * b).astype(half)
-        for n, zz in enumerate(order):
-            product = jnp.dot(hidden[part, :], down_all[:, lanes(zz * width, width)], preferred_element_type=f32)
-            for j in range(2):
-                partial[1, 2 * zz + j, part, :] = product[:, j * block:(j + 1) * block].astype(half)
-            for j in range(2):
-                block_send(1, 2 * zz + j, h)
-            if n > 1:
+        for c, (first, count) in enumerate(cuts[h]):
+            base = sides[h] * rows + first
+            part = subs(base, count)
+            lax.fori_loop(0, count // 128, norm_rows(first_all, 4, base), 0)
+            mix(base, count)
+            lax.fori_loop(0, count // 128, norm_rows(mixed_all, 5, base), 0)
+            a = jnp.dot(normed[part, :], gate_all[...], preferred_element_type=f32) * vector(6, upper(z) * small, big)
+            b = jnp.dot(normed[part, :], up_all[...], preferred_element_type=f32) * vector(7, upper(z) * small, big)
+            hidden[part, :] = (a / (1.0 + jnp.exp(-a)) * b).astype(half)
+            for n, zz in enumerate(order):
+                product = jnp.dot(hidden[part, :], down_all[:, lanes(zz * width, width)], preferred_element_type=f32)
                 for j in range(2):
-                    second_sum(2 * zz + j, h)
+                    partial[2 * zz + j, part, :] = product[:, j * block:(j + 1) * block].astype(half)
+                for j in range(2):
+                    part_send(2 * zz + j, h, c, base, count)
+                if n > 1:
+                    for j in range(2):
+                        part_sum(2 * zz + j, h, c, base, first, count)
 
     for j in range(2):
-        for k in range(3):
-            arrive(shares.at[1, k, j], rs_recv.at[1, k, j])
-
-        def target(at, here, total, j=j):
-            value = mixed_all[here, lanes(tp * width + j * block, block)].astype(f32)
-            factor = 0.5 * vector(2, j * block, block)
-            out[pl.ds(at, 64), j * block:(j + 1) * block] = (value + total * factor).astype(half)
-        add_rows(2 * tp + j, 1, ((0, j), (1, j), (2, j)), target)
-
-    for make, cond in ends:
-        if cond is None:
-            make().wait_send()
-        else:
-            pl.when(cond)(lambda make=make: make().wait_send())
+        for k, h in ((0, 1), (1, 0), (2, 0)):
+            for c, (first, count) in enumerate(cuts[h]):
+                arrive(shares.at[k, j, pl.ds(first, count)], rs_recv.at[k, j, c])
+        f = 2 * tp + j
+
+        def total_rows(i, carry, j=j, f=f):
+            at = pl.multiple_of(i * 128, 128)
+            here = pl.ds(pl.multiple_of(low * rows + at, 128), 128)
+            total = partial[f, here, :].astype(f32)
+            for k in range(3):
+                total = total + shares[k, j, pl.ds(at, 128), :].astype(f32)
+            value = mixed_all[here, lanes(f * block, block)].astype(f32)
+            out[pl.ds(at, 128), j * block:(j + 1) * block] = (
+                value + total * (0.5 * vector(2, j * block, block))).astype(half)
+            return carry
+        lax.fori_loop(0, rows // 128, total_rows, 0)
+
+    flush()
 
 
 def fits(nfs, ntp, stream, gate, pool_in):
@@ -978,13 +1034,13 @@
     tiles = gate.shape[1] // 128
     return (
         (ny, nz, ntp) == (2, 4, 4) and gate.shape[1] % 128 == 0 and tiles % 2 == 1 and tiles > 1
-        and stream.shape[0] % SEQ == 0 and stream.shape[0] % 128 == 0 and pool_in.shape[1] % 128 == 0
+        and stream.shape[0] % SEQ == 0 and stream.shape[0] > SEQ and SEQ % 128 == 0 and pool_in.shape[1] % 128 == 0
         and gate.shape[0] % 128 == 0 and stream.shape[1] == 2 * gate.shape[0]
-        and 2 * stream.shape[0] % 256 == 0
     )
 
 
-def whole_layer(stream, gate, up, down, pool_in, pool_out, vectors):
+def whole_layer(stream, weights, vectors):
+    gate, up, down, pool_in, pool_out = weights
     rows, width = stream.shape
     block, units = gate.shape
     chans = pool_in.shape[1]
@@ -995,16 +1051,16 @@
     every = 2 * rows
     f32, half = jnp.float32, jnp.bfloat16
     vmem = pl.BlockSpec(memory_space=pltpu.VMEM)
-    hbm = pl.BlockSpec(memory_space=pl.ANY)
+    hbm = pl.BlockSpec(memory_space=pltpu.HBM)
     dma = pltpu.SemaphoreType.DMA
-    weights = (gate, up, down, pool_in, pool_out)
     return pl.pallas_call(
         functools.partial(layer_kernel, (rows, small, extra)),
         name="whole_layer",
         out_shape=jax.ShapeDtypeStruct((rows, width), half),
-        in_specs=[hbm] * 6 + [vmem],
+        in_specs=[hbm] * (1 + len(weights) + len(vectors)),
         out_specs=vmem,
-        scratch_shapes=[pltpu.VMEM(w.shape, half) for w in weights] + [pltpu.VMEM(w.shape, f32) for w in weights] + [
+        scratch_shapes=[pltpu.VMEM((1, sum(v.shape[0] for v in vectors)), f32)] + [
+            pltpu.VMEM(w.shape, half) for w in weights] + [pltpu.VMEM(w.shape, f32) for w in weights] + [
             pltpu.VMEM((features, big), half), pltpu.VMEM((features, big), half), pltpu.VMEM((big, features), half),
             pltpu.VMEM((features, 4 * chans), half), pltpu.VMEM((4 * chans, features), half),
             pltpu.VMEM((4, 1, chans + 2 * width), f32),
@@ -1012,16 +1068,17 @@
             pltpu.VMEM((every, features), half), pltpu.VMEM((every, features), half),
             pltpu.VMEM((every, big), f32), pltpu.VMEM((every, big), f32), pltpu.VMEM((every, big), half),
             pltpu.VMEM((rows, 4 * chans), half),
-            pltpu.VMEM((2, 8, every, block), half), pltpu.VMEM((2, 4, every, block), half),
-            pltpu.VMEM((2, 3, 2, rows, block), half),
-            dma((5,)), dma((10,)), dma((4, 3, 2)), dma((4, 3, 2)), dma((8, 3, 2)),
+            pltpu.VMEM((8, every, block), half), pltpu.VMEM((2, 4, every, block), half),
+            pltpu.VMEM((3, 2, rows, block), half), pltpu.VMEM((2, 4, rows, block), half),
+            dma((5,)), dma((len(vectors),)), dma((10,)), dma((4, 3, 2)), dma((4, 3, 2)), dma((8, 3, 2)),
             dma((2, 4)), dma((2, 4)), dma((2, 8)), dma((2, 3)), dma((2, 4)),
             dma((3,)), dma((4,)), dma((2, 2, 7)), dma((2, 2, 4, 2)),
-            dma((2, 8, 2)), dma((2, 4, 2)), dma((2, 4, 3)), dma((2, 3, 2)),
+            dma((8, 2)), dma((4, 2)), dma((8, 2, 2)), dma((4, 2, 2)), dma((4, 3, 2)), dma((3, 2, 2)),
+            dma((4, 5)), dma((4, 3)), dma((4, 2)),
         ],
         compiler_params=pltpu.CompilerParams(
-            collective_id=0, has_side_effects=True, vmem_limit_bytes=60 << 20),
-    )(stream, *weights, vectors)
+            collective_id=0, has_side_effects=True, vmem_limit_bytes=55 << 20),
+    )(stream, *weights, *vectors)
 
 
 def body(
@@ -1032,10 +1089,9 @@
 ):
     half = jnp.bfloat16
     if fits(nfs, ntp, stream, gate_weight, pool_in_weight):
-        vectors = jnp.concatenate([
-            pool_in_scale, pool_out_scale, down_scale, gain_first, gain_mixer, gain_second, gate_scale, up_scale])
         return whole_layer(
-            stream, gate_weight, up_weight, down_weight, pool_in_weight, pool_out_weight, vectors.reshape(1, -1))
+            stream, (gate_weight, up_weight, down_weight, pool_in_weight, pool_out_weight),
+            (pool_in_scale, pool_out_scale, down_scale, gain_first, gain_mixer, gain_second, gate_scale, up_scale))
     in_half, out_half = pool_in_weight.astype(half), pool_out_weight.astype(half)
     width, channels = stream.shape[1], in_half.shape[1]
     scales = jnp.concatenate([pool_in_scale, pool_out_scale]).reshape(1, -1)

time: 204 us -> 180 us (0.88); the launches traced: 200 us -> 179 us
  Pallas kernels: 192 us -> 178 us
  local copies, waits for them, and re-layouts: 7.96 us -> 1.77 us
    pallas_call x1, Pallas kernels: 192 us -> 178 us  [whole_layer(): pl.pallas_call(functools.partial(layer_kernel, (rows, small, extra)), nam...]
    unnamed x8 -> x1, local copies, waits for them, and re-layouts: 6.61 us -> 1.77 us
where the time goes in v3:
time: 180 us; the launch traced here: 179 us
  Pallas kernels  178 us (99%)
    pallas_call x1, Pallas kernels, whole_layer(): pl.pallas_call(functools.partial(layer_kernel, (rows, small, extra)), nam...  178 us

profile of v3, /device:TPU:0, one launch (start us, length us, event | category | flops | bytes accessed | tf_op | source)
XLA Modules:
  0.0 179.4 jit_solution(1798970993873692951)
XLA Ops:
  0.0 177.6 %whole_layer.1 = bf16[384,512]{1,0:T(8,128)(2,1)} custom-call(bf16[384,512]{1,0:T(8,128)(2,1)} %stream.1, f32[256,1408]{1,0:T(8,128)} %gate_in.1, f32[256,1408]{1,0:T(8,128)} %up_in.1, f32[1408,256]{1,0:T(8,128)} %down_in.1, f32[256,128]{1,0:T(8,128)} %in_in.1, f32[128,256]{1,0:T(8,128)} %out_in.1, f32[128]{0:T(128)} %refs_0_.1, f32[512]{0:T(512)} %refs_1_.1, ...), custom_call_target="tpu_custom_call" | custom-call | tf_op jit(solution)/shard_map/whole_layer/pallas_call | solution.py:1056
  177.6 1.8 copy.16

commit v4 on v3

--- a/solution.py
+++ b/solution.py
@@ -12,7 +12,7 @@
 
 eps = 1e-06
 WINDOWS = (2, 4, 8, 16)
-Z_FIRST = (5, 7)
+Z_FIRST = (3, 5, 7)
 
 
 def fs_grid(count):
@@ -638,26 +638,40 @@
     for which, own in enumerate((pool_in, pool_out)):
         locals_.append(pltpu.make_async_copy(own, pool_place(which, fs, tp), local_sem.at[2 + which]))
 
+    PARTS = 3
+
     def own_part(piece, part, side):
-        first, count = (side * small, small) if part == 0 else (2 * small, extra)
-        ref = (gate, up, down)[piece]
-        return ref.at[subs(first, count)] if piece == 2 else ref.at[:, lanes(first, count)]
+        first = 2 * small if part == 2 else side * small
+        if piece == 2:
+            return down.at[subs(first + part % 2 * (small // 2), extra if part == 2 else small // 2)]
+        ref = (gate, up)[piece]
+        if part == 2:
+            return ref.at[:, lanes(first, extra)]
+        return ref.at[pl.ds(part * (block // 2), block // 2), lanes(first, small)]
 
     def all_part(piece, part, f):
-        first, count = (0, small) if part == 0 else (small, extra)
         if piece == 2:
-            return down_all.at[pl.ds(first, count), lanes(f * block, block)]
-        return (gate_all, up_all)[piece].at[subs(f * block, block), pl.ds(first, count)]
+            at, count = (small, extra) if part == 2 else (part * (small // 2), small // 2)
+            return down_all.at[pl.ds(at, count), lanes(f * block, block)]
+        ref = (gate_all, up_all)[piece]
+        if part == 2:
+            return ref.at[subs(f * block, block), pl.ds(small, extra)]
+        return ref.at[subs(f * block + part * (block // 2), block // 2), pl.ds(0, small)]
+
+    def part_cond(part, wide, cond=None):
+        if part < 2:
+            return cond
+        return wide == 1 if cond is None else cond & (wide == 1)
 
     def y_own(piece):
-        for part in range(2):
+        for part in range(PARTS):
             start(lambda part=part: remote(
                 own_part(piece, part, upper(z)), all_part(piece, part, fs), y_send.at[0, piece, part],
-                w_recv.at[fs, piece, part], fs_y, tp), None if part == 0 else upper(z) == 1)
+                w_recv.at[fs, piece, part], fs_y, tp), part_cond(part, upper(z)))
 
     def own_copy(piece, part):
         return pltpu.make_async_copy(
-            own_part(piece, part, upper(z)), all_part(piece, part, fs), local_sem.at[4 + 2 * piece + part])
+            own_part(piece, part, upper(z)), all_part(piece, part, fs), local_sem.at[4 + PARTS * piece + part])
 
     for copy in locals_:
         copy.start()
@@ -666,10 +680,8 @@
     def z_own(piece, cond=None, targets=(1, 2, 3)):
         for k in targets:
             at = zs[k]
-            for part in range(2):
-                ok = cond
-                if part:
-                    ok = upper(at) == 1 if cond is None else cond & (upper(at) == 1)
+            for part in range(PARTS):
+                ok = part_cond(part, upper(at), cond)
                 start(lambda k=k, at=at, part=part: remote(
                     own_part(piece, part, upper(at)), all_part(piece, part, fs), z_send.at[k, piece, part],
                     w_recv.at[fs, piece, part], 2 * at + y, tp), ok)
@@ -683,10 +695,12 @@
     z_own(1, inner, (1,))
     z_own(1, None, (2, 3))
     y_own(1)
+    y_own(2)
     z_own(2, None, (1,))
     for piece in range(3):
         own_copy(piece, 0).start()
-        pl.when(upper(z) == 1)(lambda piece=piece: own_copy(piece, 1).start())
+        own_copy(piece, 1).start()
+        pl.when(upper(z) == 1)(lambda piece=piece: own_copy(piece, 2).start())
 
     @pl.when(upper(z) == 0)
     def _():
@@ -695,20 +709,22 @@
         down_all[small:big, :] = jnp.zeros((extra, features), half)
 
     def weights_here(piece, f):
-        arrive(all_part(piece, 0, f), w_recv.at[f, piece, 0])
-        arrive(all_part(piece, 1, f), w_recv.at[f, piece, 1], upper(z) == 1)
+        for part in range(PARTS):
+            arrive(all_part(piece, part, f), w_recv.at[f, piece, part], part_cond(part, upper(z)))
 
     def by_z(piece, i):
         f = 2 * zs[i] + y
-        weights_here(piece, f)
-        for part in range(2):
+        for part in range(PARTS):
+            cond = part_cond(part, upper(z))
+            arrive(all_part(piece, part, f), w_recv.at[f, piece, part], cond)
             start(lambda part=part: remote(
                 all_part(piece, part, f), all_part(piece, part, f), y_send.at[i, piece, part],
-                w_recv.at[f, piece, part], fs_y, tp), None if part == 0 else upper(z) == 1)
+                w_recv.at[f, piece, part], fs_y, tp), cond)
 
     def own_here(piece):
         own_copy(piece, 0).wait()
-        pl.when(upper(z) == 1)(lambda: own_copy(piece, 1).wait())
+        own_copy(piece, 1).wait()
+        pl.when(upper(z) == 1)(lambda: own_copy(piece, 2).wait())
 
     step = 32
     lane_tiles = features // 128
@@ -777,13 +793,11 @@
             accumulate(weights, total, g, False)
             if (piece, i) == (0, 2):
                 pool_by_y()
-            if (piece, i) == (0, 3):
-                y_own(2)
             if (piece, i) == (1, 0):
-                z_own(2, outer, (2, 3))
+                z_own(2, inner, (2, 3))
                 pool_across()
             if (piece, i) == (1, 1):
-                z_own(2, inner, (2, 3))
+                z_own(2, outer, (2, 3))
     own_here(2)
 
     def hide(i, carry):
@@ -817,7 +831,8 @@
                 return carry
             lax.fori_loop(0, rows // 128, one, 0)
 
-    blocks = [2 * zs[i] + j for i in range(4) for j in (y, 1 - y)]
+    pair_z = (jnp.where(low == core, zp, z), jnp.where(low == core, z, zp), zs[2], zs[3])
+    blocks = [2 * zz + j for zz in pair_z for j in (y, 1 - y)]
 
     def ways(n):
         across_x, across_z = (fs, tp_x), (fs_z, tp)
@@ -930,30 +945,30 @@
     locals_[0].wait()
     for t in (tp_c, tp_x, tp_xc):
         arrive(scales_all.at[t], sc_recv.at[t])
-    for n, f in enumerate(blocks):
+    def product_of(n):
+        f = blocks[n]
         if n % 2:
             weights_here(2, f)
         partial[f, :, :] = jnp.dot(
             hidden[...], down_all[:, lanes(f * block, block)], preferred_element_type=f32).astype(half)
         for r in (1 - ways(n)[2], ways(n)[2]):
             block_send(f, r)
-        first_sum(n)
-        if n == 2:
-            slab_across()
-        if n in (3, 4):
-            by_z(2, n - 1)
-        for stage, members in {
-            1: ((first_add, (0,)),), 2: ((first_add, (1,)),), 3: ((first_add, (2, 3)),),
-            4: ((first_done, (0, 2, 1, 3)),), 5: ((first_add, (4,)), (first_pass, (0, 2))),
-            6: ((first_add, (5,)), (first_pass, (1, 3))), 7: ((first_done, (4,)), (first_add, (6, 7))),
-        }.get(n, ()):
-            for m in members:
-                stage(m)
-    for stage, m in (
-        (first_done, 5), (first_pass, 4), (first_done, 6), (first_pass, 5), (first_done, 7), (first_pass, 6),
-        (first_pass, 7),
+
+    def down_from(n):
+        by_z(2, n)
+
+    def slab(n):
+        slab_across()
+
+    for stage, members in (
+        (product_of, (0, 1, 2, 3)), (first_sum, (2, 3)), (slab, (0,)), (first_add, (2, 3)), (down_from, (2,)),
+        (product_of, (4,)), (down_from, (3,)), (product_of, (6,)), (first_sum, (4, 6)), (first_done, (2, 3)),
+        (first_add, (4, 6)), (product_of, (5,)), (first_sum, (5,)), (first_pass, (2, 3)), (first_done, (4, 6)),
+        (product_of, (7,)), (first_sum, (7,)), (first_add, (5,)), (first_pass, (4, 6)), (first_done, (5,)),
+        (first_add, (7,)), (first_pass, (5,)), (first_done, (7,)), (first_pass, (7,)),
     ):
-        stage(m)
+        for m in members:
+            stage(m)
     for which in range(2):
         for t in (tp_c, tp_xc):
             arrive(pool_slab(which, t), slab_recv.at[which, t])
@@ -1070,7 +1085,7 @@
             pltpu.VMEM((rows, 4 * chans), half),
             pltpu.VMEM((8, every, block), half), pltpu.VMEM((2, 4, every, block), half),
             pltpu.VMEM((3, 2, rows, block), half), pltpu.VMEM((2, 4, rows, block), half),
-            dma((5,)), dma((len(vectors),)), dma((10,)), dma((4, 3, 2)), dma((4, 3, 2)), dma((8, 3, 2)),
+            dma((5,)), dma((len(vectors),)), dma((13,)), dma((4, 3, 3)), dma((4, 3, 3)), dma((8, 3, 3)),
             dma((2, 4)), dma((2, 4)), dma((2, 8)), dma((2, 3)), dma((2, 4)),
             dma((3,)), dma((4,)), dma((2, 2, 7)), dma((2, 2, 4, 2)),
             dma((8, 2)), dma((4, 2)), dma((8, 2, 2)), dma((4, 2, 2)), dma((4, 3, 2)), dma((3, 2, 2)),

time: 180 us -> 179 us (level)
  Pallas kernels: 178 us -> 176 us
where the time goes in v4:
time: 179 us; the launch traced here: 178 us
  Pallas kernels  176 us (98%)
    pallas_call x1, Pallas kernels, whole_layer(): pl.pallas_call(functools.partial(layer_kernel, (rows, small, extra)), nam...  176 us

profile of v4, /device:TPU:0, one launch (start us, length us, event | category | flops | bytes accessed | tf_op | source)
XLA Modules:
  0.0 178.2 jit_solution(15019785473349451180)
XLA Ops:
  0.0 176.5 %whole_layer.1 = bf16[384,512]{1,0:T(8,128)(2,1)} custom-call(bf16[384,512]{1,0:T(8,128)(2,1)} %stream.1, f32[256,1408]{1,0:T(8,128)} %gate_in.1, f32[256,1408]{1,0:T(8,128)} %up_in.1, f32[1408,256]{1,0:T(8,128)} %down_in.1, f32[256,128]{1,0:T(8,128)} %in_in.1, f32[128,256]{1,0:T(8,128)} %out_in.1, f32[128]{0:T(128)} %refs_0_.1, f32[512]{0:T(512)} %refs_1_.1, ...), custom_call_target="tpu_custom_call" | custom-call | tf_op jit(solution)/shard_map/whole_layer/pallas_call | solution.py:1071
  176.5 1.8 copy.16

commit v5 on v4

--- a/solution.py
+++ b/solution.py
@@ -529,7 +529,7 @@
             return carry
         lax.fori_loop(0, count // each, one, 0)
 
-    for load in loads:
+    for load in loads[:3]:
         narrowed(*load)
     stream_own.wait()
     for copy in vector_copies:
@@ -550,13 +550,13 @@
             pl.when(cond)(lambda: make().start())
         ends.append((make, cond))
 
-    def flush():
-        for make, cond in ends:
+    def flush(count=None):
+        for make, cond in ends[:count]:
             if cond is None:
                 make().wait_send()
             else:
                 pl.when(cond)(lambda make=make: make().wait_send())
-        ends.clear()
+        del ends[:count]
 
     def arrive(dst, recv, cond=None):
         def wait():
@@ -689,6 +689,8 @@
     outer = jnp.logical_not(inner)
     z_own(0, None, (1,))
     y_own(0)
+    for load in loads[3:]:
+        narrowed(*load)
     z_own(1, outer, (1,))
     z_own(0, None, (2, 3))
     pool_start()
@@ -780,6 +782,7 @@
                 start(lambda which=which, slab=slab, n=n, t=t: remote(
                     slab, slab, slab_send.at[which, n], slab_recv.at[which, tp], fs, t))
 
+    early_sends = len(ends)
     ahead = [(piece, i) for piece in range(3) for i in range(1, 4)]
     for piece, (weights, total) in enumerate(((gate_all, gate_sum), (up_all, up_sum))):
         for i in range(4):
@@ -959,6 +962,7 @@
 
     def slab(n):
         slab_across()
+        flush(early_sends)
 
     for stage, members in (
         (product_of, (0, 1, 2, 3)), (first_sum, (2, 3)), (slab, (0,)), (first_add, (2, 3)), (down_from, (2,)),
@@ -972,8 +976,8 @@
     for which in range(2):
         for t in (tp_c, tp_xc):
             arrive(pool_slab(which, t), slab_recv.at[which, t])
+    flush()
     first_finish()
-    flush()
 
     in_scale = jnp.concatenate([scales_all[t, :, :chans] for t in range(4)], axis=1)
     group = 4 * chans // 4
@@ -981,9 +985,27 @@
     pos_col = lax.broadcasted_iota(jnp.int32, (SEQ, SEQ), 1)
     pos = lax.broadcasted_iota(jnp.int32, (SEQ, 1), 0)
 
+    def row_scale(total):
+        return lax.rsqrt(jnp.sum(total, axis=-1, keepdims=True) * (1.0 / features) + eps)
+
+    def gained_rows(base, count):
+        scale = []
+        for i in range(count // 128):
+            part = pl.ds(pl.multiple_of(base + i * 128, 128), 128)
+            total = jnp.zeros((128, 128), f32)
+            for c in range(lane_tiles):
+                cols = slice(c * 128, (c + 1) * 128)
+                floats = first_all[part, cols].astype(f32)
+                total = total + floats * floats
+                normed[part, cols] = (floats * vector(4, c * 128, 128)).astype(half)
+            scale.append(row_scale(total))
+        return jnp.concatenate(scale, axis=0)
+
     def mix(base, count):
+        scale = gained_rows(base, count)
         part = pl.ds(pl.multiple_of(base, 128), count)
-        pool_input = (jnp.dot(normed[part, :], in_all[...], preferred_element_type=f32) * in_scale).astype(half)
+        pool_input = (
+            jnp.dot(normed[part, :], in_all[...], preferred_element_type=f32) * scale * in_scale).astype(half)
         for index, window in enumerate(WINDOWS):
             before = window // 2
             first = jnp.maximum(pos_row - before, 0)
@@ -995,11 +1017,18 @@
                 sums = jnp.dot(members, own, preferred_element_type=f32)
                 pooled[s * SEQ:(s + 1) * SEQ, index * group:(index + 1) * group] = (
                     sums / counts - own.astype(f32)).astype(half)
+        total = jnp.zeros((count, 128), f32)
         for t in range(4):
             cols = slice(t * width, (t + 1) * width)
             mixed = jnp.dot(pooled[:count, :], out_all[:, cols], preferred_element_type=f32)
-            mixed_all[part, cols] = (
-                first_all[part, cols].astype(f32) + mixed * scales_all[t, :, chans:chans + width]).astype(half)
+            value = (first_all[part, cols].astype(f32) + mixed * scales_all[t, :, chans:chans + width]).astype(half)
+            mixed_all[part, cols] = value
+            value = value.astype(f32)
+            normed[part, cols] = (value * vector(5, t * width, width)).astype(half)
+            for c in range(width // 128):
+                tile_of = value[:, c * 128:(c + 1) * 128]
+                total = total + tile_of * tile_of
+        return row_scale(total)
 
     order = [2 * xx + cc for cc in (1 - core, core) for xx in (1 - x, x)]
     sides = (1 - low, low)
@@ -1007,11 +1036,9 @@
         for c, (first, count) in enumerate(cuts[h]):
             base = sides[h] * rows + first
             part = subs(base, count)
-            lax.fori_loop(0, count // 128, norm_rows(first_all, 4, base), 0)
-            mix(base, count)
-            lax.fori_loop(0, count // 128, norm_rows(mixed_all, 5, base), 0)
-            a = jnp.dot(normed[part, :], gate_all[...], preferred_element_type=f32) * vector(6, upper(z) * small, big)
-            b = jnp.dot(normed[part, :], up_all[...], preferred_element_type=f32) * vector(7, upper(z) * small, big)
+            scale = mix(base, count)
+            a = jnp.dot(normed[part, :], gate_all[...], preferred_element_type=f32) * scale * vector(6, upper(z) * small, big)
+            b = jnp.dot(normed[part, :], up_all[...], preferred_element_type=f32) * scale * vector(7, upper(z) * small, big)
             hidden[part, :] = (a / (1.0 + jnp.exp(-a)) * b).astype(half)
             for n, zz in enumerate(order):
                 product = jnp.dot(hidden[part, :], down_all[:, lanes(zz * width, width)], preferred_element_type=f32)
@@ -1023,6 +1050,7 @@
                     for j in range(2):
                         part_sum(2 * zz + j, h, c, base, first, count)
 
+    flush()
     for j in range(2):
         for k, h in ((0, 1), (1, 0), (2, 0)):
             for c, (first, count) in enumerate(cuts[h]):
@@ -1040,8 +1068,6 @@
                 value + total * (0.5 * vector(2, j * block, block))).astype(half)
             return carry
         lax.fori_loop(0, rows // 128, total_rows, 0)
-
-    flush()
 
 
 def fits(nfs, ntp, stream, gate, pool_in):
@@ -1092,7 +1118,7 @@
             dma((4, 5)), dma((4, 3)), dma((4, 2)),
         ],
         compiler_params=pltpu.CompilerParams(
-            collective_id=0, has_side_effects=True, vmem_limit_bytes=55 << 20),
+            collective_id=0, has_side_effects=True, vmem_limit_bytes=54 << 20),
     )(stream, *weights, *vectors)
 
 

time: 179 us -> 178 us (level)
  Pallas kernels: 176 us -> 174 us
    pallas_call x1, Pallas kernels: 176 us -> 174 us  [whole_layer(): pl.pallas_call(functools.partial(layer_kernel, (rows, small, extra)), nam...]
where the time goes in v5:
time: 178 us; the launch traced here: 176 us
  Pallas kernels  174 us (98%)
    pallas_call x1, Pallas kernels, whole_layer(): pl.pallas_call(functools.partial(layer_kernel, (rows, small, extra)), nam...  174 us

profile of v5, /device:TPU:0, one launch (start us, length us, event | category | flops | bytes accessed | tf_op | source)
XLA Modules:
  0.0 175.7 jit_solution(3060608619713244675)
XLA Ops:
  0.0 173.9 %whole_layer.1 = bf16[384,512]{1,0:T(8,128)(2,1)} custom-call(bf16[384,512]{1,0:T(8,128)(2,1)} %stream.1, f32[256,1408]{1,0:T(8,128)} %gate_in.1, f32[256,1408]{1,0:T(8,128)} %up_in.1, f32[1408,256]{1,0:T(8,128)} %down_in.1, f32[256,128]{1,0:T(8,128)} %in_in.1, f32[128,256]{1,0:T(8,128)} %out_in.1, f32[128]{0:T(128)} %refs_0_.1, f32[512]{0:T(512)} %refs_1_.1, ...), custom_call_target="tpu_custom_call" | custom-call | tf_op jit(solution)/shard_map/whole_layer/pallas_call | solution.py:1097
  173.9 1.8 %copy.16 = bf16[384,512]{1,0:T(8,128)(2,1)} copy(bf16[384,512]{1,0:T(8,128)(2,1)} %whole_layer.1) | data formatting | bytes 786432

commit v6 on v5

--- a/solution.py
+++ b/solution.py
@@ -797,10 +797,10 @@
             if (piece, i) == (0, 2):
                 pool_by_y()
             if (piece, i) == (1, 0):
-                z_own(2, inner, (2, 3))
+                z_own(2, outer, (2, 3))
                 pool_across()
             if (piece, i) == (1, 1):
-                z_own(2, outer, (2, 3))
+                z_own(2, inner, (2, 3))
     own_here(2)
 
     def hide(i, carry):

time: 178 us -> 176 us (0.989); the launches traced: 176 us -> 176 us
  no operation moved by 1% of the time
where the time goes in v6:
time: 176 us
  Pallas kernels  174 us (99%)
  local copies, waits for them, and re-layouts  1.77 us (1%)
    pallas_call x1, Pallas kernels, whole_layer(): pl.pallas_call(functools.partial(layer_kernel, (rows, small, extra)), nam...  174 us

profile of v6, /device:TPU:0, one launch (start us, length us, event | category | flops | bytes accessed | tf_op | source)
XLA Modules:
  0.0 175.6 jit_solution(17505009872111871092)
XLA Ops:
  0.0 173.8 %whole_layer.1 = bf16[384,512]{1,0:T(8,128)(2,1)} custom-call(bf16[384,512]{1,0:T(8,128)(2,1)} %stream.1, f32[256,1408]{1,0:T(8,128)} %gate_in.1, f32[256,1408]{1,0:T(8,128)} %up_in.1, f32[1408,256]{1,0:T(8,128)} %down_in.1, f32[256,128]{1,0:T(8,128)} %in_in.1, f32[128,256]{1,0:T(8,128)} %out_in.1, f32[128]{0:T(128)} %refs_0_.1, f32[512]{0:T(512)} %refs_1_.1, ...), custom_call_target="tpu_custom_call" | custom-call | tf_op jit(solution)/shard_map/whole_layer/pallas_call | solution.py:1097
  173.8 1.8 %copy.16 = bf16[384,512]{1,0:T(8,128)(2,1)} copy(bf16[384,512]{1,0:T(8,128)(2,1)} %whole_layer.1) | data formatting | bytes 786432
